TPU v7x, 32 devices: a whole 2x2x4 slice. The times are simulated.
32 devices in a mesh: ep: 8 (over z, y), tp: 4 (over x, core).
Axes of the slice: x: 2, y: 2, z: 4, core: 2. Of those that a mesh axis runs over, the one named last changes fastest.
Arguments:
- queries: bfloat16 [2048, 1536], P('ep', 'tp'), may hold values from -6 to 6
- kv_latent: bfloat16 [2048, 512], P('ep'), may hold values from -6 to 6
- rope_key: bfloat16 [2048, 64], P('ep'), may hold values from -6 to 6
- latent_gain: float32 [512], replicated, may hold values from 0.1 to 1.9
- w_key_up: bfloat16 [512, 1024], P(None, 'tp'), may hold values from -0.25 to 0.25
- w_value_up: bfloat16 [512, 1024], P(None, 'tp'), may hold values from -0.25 to 0.25
- query_gain: float32 [192], replicated, may hold values from 0.1 to 1.9
- key_gain: float32 [128], replicated, may hold values from 0.1 to 1.9
- rope_gain: float32 [64], replicated, may hold values from 0.1 to 1.9
- out_gain: float32 [128], replicated, may hold values from 0.1 to 1.9
- moe_tokens: bfloat16 [2048, 2048], P('ep'), may hold values from -6 to 6
- moe_gain: float32 [2048], replicated, may hold values from 0.1 to 1.9
- routes: int32 [2048, 2], P('ep'), may hold values from 0 to 7, all different within a row; in each aligned block of 64 rows (0 to 63, 64 to 127, ...) at most 24 rows name the same one
- route_weights: float32 [2048, 2], P('ep'), may hold values from 0.25 to 1
- w_gate: bfloat16 [8, 2048, 3584], P('ep', None, 'tp'), may hold values from -0.125 to 0.125
- w_up: bfloat16 [8, 2048, 3584], P('ep', None, 'tp'), may hold values from -0.125 to 0.125
- w_down: bfloat16 [8, 3584, 2048], P('ep', 'tp'), may hold values from -0.09375 to 0.09375
Outputs:
- attended: bfloat16 [2048, 1024], P('ep', 'tp')
- moe_out: bfloat16 [2048, 2048], P(('ep', 'tp'))
Inputs may be any that keep to these rules, and one draw needn't show every extreme that they name: `routes`: each row names 2 different experts of 0 to 7; in each aligned block of 64 rows no expert is named by more than 24 rows, and in some block one expert is named by exactly 24.
All inputs are finite; a program needn't handle non-finite values.
Results may differ from a plain program's by a relative error of at most 0.0071.
Values may be sent and summed in bfloat16 or wider, within the bound.
A program may use at most 128 MiB of HBM per device.

v0:
```python
import functools
import math

import jax
import jax.numpy as jnp
from jax import lax
from jax.experimental import pallas as pl
from jax.experimental.pallas import tpu as pltpu
from jax.sharding import PartitionSpec as P

EPS = 1e-06
THETA = 500000.0


def rms_norm(values, norm_gain):
    return values * lax.rsqrt(jnp.mean(values * values, axis=-1, keepdims=True) + EPS) * norm_gain


def rope_tables(positions, rope_dim):
    freqs = 1.0 / THETA ** (jnp.arange(0, rope_dim, 2, dtype=jnp.float32) / rope_dim)
    angles = positions.astype(jnp.float32)[:, None] * freqs[None, :]
    return (jnp.cos(angles), jnp.sin(angles))


def rotate(values, rot_cos, rot_sin):
    half_dim = values.shape[-1] // 2
    first_half = values[..., :half_dim]
    second_half = values[..., half_dim:]
    return jnp.concatenate(
        [
            first_half * rot_cos - second_half * rot_sin,
            second_half * rot_cos + first_half * rot_sin,
        ],
        axis=-1,
    )

MESH = pl.DeviceIdType.MESH
VMEM = pltpu.VMEM


def remote(src, dst, send, recv, device):
    return pltpu.make_async_remote_copy(
        src_ref=src, dst_ref=dst, send_sem=send, recv_sem=recv, device_id=device, device_id_type=MESH
    )


def greet(me, quarter, n_ep, highs):
    high, low = quarter // 2, quarter % 2
    barrier = pltpu.get_barrier_semaphore()

    def hello(device):
        pl.semaphore_signal(barrier, inc=1, device_id=device, device_id_type=MESH)

    def hello_ep(step, carry):
        hello((lax.rem(me + step, n_ep), quarter))
        return carry

    lax.fori_loop(1, n_ep, hello_ep, 0)
    hello((me, high * 2 + 1 - low))
    for step in range(1, highs):
        hello((me, lax.rem(high + step, highs) * 2 + low))
    pl.semaphore_wait(barrier, n_ep - 1 + 1 + highs - 1)


def spread_kernel(
    n_ep, highs, rows_ref, lat_ref, arrived, lat_all,
    own_sem, ep_send, ep_recv, high_send, high_recv, low_send, low_recv,
):
    me, quarter = lax.axis_index("ep"), lax.axis_index("tp")
    high, low = quarter // 2, quarter % 2
    partner = (me, high * 2 + 1 - low)
    greet(me, quarter, n_ep, highs)
    payloads = (
        (lambda j: rows_ref.at[j], arrived),
        (lambda j: lat_ref, lat_all),
    )
    own = [
        pltpu.make_async_copy(outgoing(me), into.at[low, high, me], own_sem.at[p])
        for p, (outgoing, into) in enumerate(payloads)
    ]
    for copy in own:
        copy.start()

    def ep_copy(p, step):
        outgoing, into = payloads[p]
        j = lax.rem(me + step, n_ep)
        return remote(
            outgoing(j), into.at[low, high, me], ep_send.at[p, step], ep_recv.at[p, step], (j, quarter)
        )

    def ep_arrival(p, step):
        outgoing, into = payloads[p]
        j = lax.rem(me + n_ep - step, n_ep)
        return remote(
            outgoing(me), into.at[low, high, j], ep_send.at[p, step], ep_recv.at[p, step], (j, quarter)
        )

    def high_copy(p, step, hop):
        into = payloads[p][1]
        j = lax.rem(me + n_ep - step, n_ep)
        block = into.at[low, high, j]
        return remote(
            block, block, high_send.at[p, hop, step], high_recv.at[p, hop, step],
            (me, lax.rem(high + hop, highs) * 2 + low),
        )

    def high_arrival(p, step, hop):
        into = payloads[p][1]
        j = lax.rem(me + n_ep - step, n_ep)
        block = into.at[low, lax.rem(high + highs - hop, highs), j]
        return remote(
            block, block, high_send.at[p, hop, step], high_recv.at[p, hop, step],
            (me, lax.rem(high + hop, highs) * 2 + low),
        )

    def low_copy(p, step, hop, side):
        into = payloads[p][1]
        j = lax.rem(me + n_ep - step, n_ep)
        block = into.at[side, lax.rem(high + highs - hop, highs), j]
        return remote(block, block, low_send.at[p, hop, step], low_recv.at[p, hop, step], partner)

    def start_ep(step, carry, p):
        ep_copy(p, step).start()
        return carry

    def forward(step, carry, p):
        ep_arrival(p, step).wait_recv()
        for hop in range(1, highs):
            high_copy(p, step, hop).start()
        low_copy(p, step, 0, low).start()
        return carry

    def forward_low(step, carry, p):
        for hop in range(1, highs):
            high_arrival(p, step, hop).wait_recv()
            low_copy(p, step, hop, low).start()
        return carry

    def finish(step, carry, p):
        for hop in range(highs):
            low_copy(p, step, hop, 1 - low).wait_recv()
            low_copy(p, step, hop, low).wait_send()
        for hop in range(1, highs):
            high_copy(p, step, hop).wait_send()
        return carry

    def finish_ep(step, carry, p):
        ep_copy(p, step).wait_send()
        return carry

    for p in range(2):
        lax.fori_loop(1, n_ep, functools.partial(start_ep, p=p), 0)
    for p in range(2):
        own[p].wait()
        for hop in range(1, highs):
            high_copy(p, 0, hop).start()
        low_copy(p, 0, 0, low).start()
        lax.fori_loop(1, n_ep, functools.partial(forward, p=p), 0)
    for p in range(2):
        lax.fori_loop(0, n_ep, functools.partial(forward_low, p=p), 0)
    for p in range(2):
        lax.fori_loop(0, n_ep, functools.partial(finish, p=p), 0)
        lax.fori_loop(1, n_ep, functools.partial(finish_ep, p=p), 0)


def spread(rows, lat, quarters):
    n_ep, cap, model_dim = rows.shape
    highs = quarters // 2
    dma = pltpu.SemaphoreType.DMA
    return pl.pallas_call(
        functools.partial(spread_kernel, n_ep, highs),
        out_shape=(
            jax.ShapeDtypeStruct((2, highs, n_ep, cap, model_dim), rows.dtype),
            jax.ShapeDtypeStruct((2, highs, n_ep) + lat.shape, lat.dtype),
        ),
        in_specs=[pl.BlockSpec(memory_space=VMEM)] * 2,
        out_specs=(pl.BlockSpec(memory_space=VMEM),) * 2,
        scratch_shapes=[
            dma((2,)),
            dma((2, n_ep)),
            dma((2, n_ep)),
            dma((2, highs, n_ep)),
            dma((2, highs, n_ep)),
            dma((2, highs, n_ep)),
            dma((2, highs, n_ep)),
        ],
        compiler_params=pltpu.CompilerParams(
            collective_id=0, has_side_effects=True, vmem_limit_bytes=60 << 20
        ),
        name="spread",
    )(rows, lat)


def collect_kernel(
    n_ep, highs, part_ref, ret, low_buf, high_buf, sum_buf, final_buf,
    low_send, low_recv, high_send, high_recv, ep_send, ep_recv,
):
    me, quarter = lax.axis_index("ep"), lax.axis_index("tp")
    high, low = quarter // 2, quarter % 2
    partner = (me, high * 2 + 1 - low)
    greet(me, quarter, n_ep, highs)

    def low_copy(step):
        j = lax.rem(me + step, n_ep)
        return remote(
            part_ref.at[1 - low, j], low_buf.at[j], low_send.at[step], low_recv.at[step], partner
        )

    def high_copy(step, hop):
        j = lax.rem(me + step, n_ep)
        other = lax.rem(high + hop, highs)
        return remote(
            sum_buf.at[j, other], high_buf.at[hop, j], high_send.at[hop, step],
            high_recv.at[hop, step], (me, other * 2 + low),
        )

    def ep_copy(step):
        j = lax.rem(me + step, n_ep)
        return remote(final_buf.at[j], ret.at[me], ep_send.at[step], ep_recv.at[step], (j, quarter))

    def ep_arrival(step):
        j = lax.rem(me + n_ep - step, n_ep)
        return remote(final_buf.at[j], ret.at[j], ep_send.at[step], ep_recv.at[step], (j, quarter))

    def start_low(step, carry):
        low_copy(step).start()
        return carry

    def add_low(step, carry):
        low_copy(step).wait_recv()
        j = lax.rem(me + step, n_ep)
        sum_buf[j] = (
            part_ref[low, j].astype(jnp.float32) + low_buf[j].astype(jnp.float32)
        ).astype(jnp.bfloat16)
        for hop in range(1, highs):
            high_copy(step, hop).start()
        return carry

    def total(step):
        j = lax.rem(me + step, n_ep)
        value = part_ref[low, j, high].astype(jnp.float32) + low_buf[j, high].astype(jnp.float32)
        for hop in range(1, highs):
            high_copy(step, hop).wait_recv()
            value = value + high_buf[hop, j].astype(jnp.float32)
        return value.astype(jnp.bfloat16)

    def add_high(step, carry):
        final_buf[lax.rem(me + step, n_ep)] = total(step)
        ep_copy(step).start()
        return carry

    def finish(step, carry):
        ep_arrival(step).wait_recv()
        ep_copy(step).wait_send()
        return carry

    def finish_tp(step, carry):
        low_copy(step).wait_send()
        for hop in range(1, highs):
            high_copy(step, hop).wait_send()
        return carry

    lax.fori_loop(1, n_ep, start_low, 0)
    low_copy(0).start()
    lax.fori_loop(1, n_ep, add_low, 0)
    add_low(0, 0)
    lax.fori_loop(1, n_ep, add_high, 0)
    ret[me] = total(0)
    lax.fori_loop(1, n_ep, finish, 0)
    lax.fori_loop(0, n_ep, finish_tp, 0)


def collect(partial):
    _, n_ep, highs, cap, model_dim = partial.shape
    dma = pltpu.SemaphoreType.DMA
    kind = partial.dtype
    return pl.pallas_call(
        functools.partial(collect_kernel, n_ep, highs),
        out_shape=jax.ShapeDtypeStruct((n_ep, cap, model_dim), kind),
        in_specs=[pl.BlockSpec(memory_space=VMEM)],
        out_specs=pl.BlockSpec(memory_space=VMEM),
        scratch_shapes=[
            VMEM((n_ep, highs, cap, model_dim), kind),
            VMEM((highs, n_ep, cap, model_dim), kind),
            VMEM((n_ep, highs, cap, model_dim), kind),
            VMEM((n_ep, cap, model_dim), kind),
            dma((n_ep,)),
            dma((n_ep,)),
            dma((highs, n_ep)),
            dma((highs, n_ep)),
            dma((n_ep,)),
            dma((n_ep,)),
        ],
        compiler_params=pltpu.CompilerParams(
            collective_id=1, has_side_effects=True, vmem_limit_bytes=62 << 20
        ),
        name="collect",
    )(partial)


def attend_kernel(
    heads, nope_dim, value_dim, latent_dim, scale,
    lat_ref, wk_ref, wv_ref, qn_ref, qr_ref, kg_ref, og_ref, out_ref, acc, den,
):
    block = pl.program_id(0)
    block_rows = lat_ref.shape[0]
    tok_rows = qn_ref.shape[1]
    offset = lax.axis_index("ep") * tok_rows
    first = block * block_rows

    @pl.when(block == 0)
    def _():
        acc[...] = jnp.zeros_like(acc)
        den[...] = jnp.zeros_like(den)

    @pl.when(first <= offset + tok_rows - 1)
    def _():
        latent = lat_ref[:, :latent_dim]
        rot_key = lat_ref[:, latent_dim:]
        keys = jnp.dot(latent, wk_ref[...], preferred_element_type=jnp.float32)
        values = jnp.dot(latent, wv_ref[...], preferred_element_type=jnp.float32).astype(jnp.bfloat16)
        shape = (tok_rows, block_rows)
        visible = offset + lax.broadcasted_iota(jnp.int32, shape, 0) >= first + lax.broadcasted_iota(
            jnp.int32, shape, 1
        )
        across = (((1,), (1,)), ((), ()))
        for head in range(heads):
            key = keys[:, head * nope_dim : (head + 1) * nope_dim]
            key = rms_norm(key, kg_ref[...]).astype(jnp.bfloat16)
            scores = lax.dot_general(qn_ref[head], key, across, preferred_element_type=jnp.float32)
            scores = scores + lax.dot_general(
                qr_ref[head], rot_key, across, preferred_element_type=jnp.float32
            )
            weights = jnp.where(visible, jnp.exp(scores * scale), 0.0)
            den[head] += jnp.sum(weights, axis=-1, keepdims=True)
            acc[head] += jnp.dot(
                weights.astype(jnp.bfloat16),
                values[:, head * value_dim : (head + 1) * value_dim],
                preferred_element_type=jnp.float32,
            )

    @pl.when(block == pl.num_programs(0) - 1)
    def _():
        for head in range(heads):
            mixed = rms_norm(acc[head] / den[head], og_ref[...])
            out_ref[:, head * value_dim : (head + 1) * value_dim] = mixed.astype(jnp.bfloat16)


def attend(lat_rows, w_key_up, w_value_up, query_nope, query_rope, key_gain, out_gain):
    heads, tok_rows, nope_dim = query_nope.shape
    rope_dim = query_rope.shape[2]
    value_dim = out_gain.shape[0]
    total, width = lat_rows.shape
    block_rows = math.gcd(total, 512)
    whole = pl.BlockSpec(memory_space=VMEM)
    return pl.pallas_call(
        functools.partial(
            attend_kernel, heads, nope_dim, value_dim, width - rope_dim, (nope_dim + rope_dim) ** (-0.5)
        ),
        grid=(total // block_rows,),
        out_shape=jax.ShapeDtypeStruct((tok_rows, heads * value_dim), jnp.bfloat16),
        in_specs=[pl.BlockSpec((block_rows, width), lambda b: (b, 0))] + [whole] * 6,
        out_specs=pl.BlockSpec((tok_rows, heads * value_dim), lambda b: (0, 0)),
        scratch_shapes=[
            VMEM((heads, tok_rows, value_dim), jnp.float32),
            VMEM((heads, tok_rows, 1), jnp.float32),
        ],
        name="attend",
    )(
        lat_rows, w_key_up, w_value_up, query_nope, query_rope,
        key_gain.reshape(1, -1), out_gain.reshape(1, -1),
    )


def on_device(
    queries,
    kv_latent,
    rope_key,
    latent_gain,
    w_key_up,
    w_value_up,
    query_gain,
    key_gain,
    rope_gain,
    out_gain,
    moe_tokens,
    moe_gain,
    routes,
    route_weights,
    w_gate,
    w_up,
    w_down,
):
    quarters = lax.axis_size("tp")
    n_ep = lax.axis_size("ep")
    my_part = lax.axis_index("tp")
    tok_rows = queries.shape[0]
    nope_dim = key_gain.shape[0]
    value_dim = out_gain.shape[0]
    rope_dim = rope_key.shape[1]
    head_count = w_key_up.shape[1] // nope_dim
    positions = lax.axis_index("ep") * tok_rows + jnp.arange(tok_rows, dtype=jnp.int32)
    rot_cos, rot_sin = rope_tables(positions, rope_dim)
    lat_part = tok_rows // quarters

    def mine(values, rows):
        return lax.dynamic_slice_in_dim(values, my_part * rows, rows, 0)

    latent = rms_norm(mine(kv_latent, lat_part).astype(jnp.float32), latent_gain)
    rot_key = rotate(
        rms_norm(mine(rope_key, lat_part).astype(jnp.float32), rope_gain),
        mine(rot_cos, lat_part),
        mine(rot_sin, lat_part),
    )
    lat_own = jnp.concatenate([latent.astype(jnp.bfloat16), rot_key.astype(jnp.bfloat16)], axis=1)

    n_rows, model_dim = moe_tokens.shape
    top_count = routes.shape[1]
    part_rows = n_rows // quarters
    experts = n_ep * w_gate.shape[0]
    capacity = (3 * top_count * part_rows + 2 * experts - 1) // (2 * experts)
    slot_count = experts * capacity
    own_rows = rms_norm(mine(moe_tokens, part_rows).astype(jnp.float32), moe_gain).astype(jnp.bfloat16)
    chosen = mine(routes, part_rows).reshape(part_rows * top_count)
    onehot = (chosen[:, None] == jnp.arange(experts, dtype=jnp.int32)).astype(jnp.float32)
    count = part_rows * top_count
    earlier = (jnp.arange(count)[:, None] > jnp.arange(count)[None, :]).astype(jnp.float32)
    rank = jnp.sum(jnp.dot(earlier, onehot) * onehot, axis=-1).astype(jnp.int32)
    slots = chosen * capacity + rank
    mine_hit = (slots[:, None] == jnp.arange(slot_count, dtype=jnp.int32)).astype(jnp.bfloat16)
    mine_hit = mine_hit.reshape(part_rows, top_count, slot_count)
    outgoing = jnp.einsum(
        "rs,rd->sd", jnp.sum(mine_hit, axis=1), own_rows, preferred_element_type=jnp.float32
    )
    outgoing = outgoing.astype(jnp.bfloat16).reshape(experts, capacity, model_dim)

    arrived, lat_all = spread(outgoing, lat_own, quarters)
    lat_rows = jnp.transpose(lat_all, (2, 1, 0, 3, 4)).reshape(n_ep * tok_rows, lat_own.shape[1])

    shape = arrived.shape
    gate = jnp.einsum("abecd,df->abecf", arrived, w_gate[0], preferred_element_type=jnp.float32)
    upward = jnp.einsum("abecd,df->abecf", arrived, w_up[0], preferred_element_type=jnp.float32)
    hidden = (jax.nn.silu(gate) * upward).astype(jnp.bfloat16)
    partial = jnp.einsum("abecf,fd->aebcd", hidden, w_down[0], preferred_element_type=jnp.float32)
    returned = collect(partial.astype(jnp.bfloat16))

    query = rms_norm(
        queries.astype(jnp.float32).reshape(tok_rows, head_count, nope_dim + rope_dim), query_gain
    )
    query_nope = query[..., :nope_dim].astype(jnp.bfloat16)
    query_rope = rotate(query[..., nope_dim:], rot_cos[:, None, :], rot_sin[:, None, :]).astype(
        jnp.bfloat16
    )
    attended = attend(
        lat_rows,
        w_key_up,
        w_value_up,
        jnp.transpose(query_nope, (1, 0, 2)),
        jnp.transpose(query_rope, (1, 0, 2)),
        key_gain,
        out_gain,
    )

    picked = jnp.einsum(
        "rks,sd->rkd",
        mine_hit,
        returned.reshape(slot_count, model_dim),
        preferred_element_type=jnp.float32,
    )
    own_weights = mine(route_weights, part_rows)
    moe_out = jnp.sum(picked * own_weights[:, :, None], axis=1).astype(jnp.bfloat16)
    return (attended, moe_out)


def solution(mesh):
    return jax.shard_map(
        on_device,
        mesh=mesh,
        in_specs=(
            P("ep", "tp"),
            P("ep", None),
            P("ep", None),
            P(),
            P(None, "tp"),
            P(None, "tp"),
            P(),
            P(),
            P(),
            P(),
            P("ep", None),
            P(),
            P("ep", None),
            P("ep", None),
            P("ep", None, "tp"),
            P("ep", None, "tp"),
            P("ep", "tp", None),
        ),
        out_specs=(P("ep", "tp"), P(("ep", "tp"), None)),
        check_vma=False,
    )
```

profile of v0, /device:TPU:0, one launch (start us, length us, event | category | flops | bytes accessed | tf_op | source)
XLA Modules:
  0.0 125.6 jit_solution(7948970193277324940)
XLA Ops:
  0.6 0.0 copy-start
  0.7 0.8 constant_dynamic-slice_fusion.2
  1.4 0.1 copy.39
  1.5 0.1 eq.51
  1.6 0.1 fusion.16
  1.8 0.1 convert_element_type.59
  2.0 0.1 copy.40
  2.0 0.8 multiply_add_fusion
  2.8 0.1 fusion.31
  2.9 1.1 fusion.17
  4.0 2.3 %convolution_convert_fusion = bf16[192,2048]{1,0:T(8,128)(2,1)} fusion(bf16[64,192]{1,0:T(8,128)(2,1)S(1)} %fusion.31, f32[2048]{0:T(1024)} %param.28, f32[64]{0:T(128)S(1)} %add_rsqrt_fusion.3, bf16[256,2048]{1,0:T(8,128)(2,1)} %param.27, s32[]{:T(128)S(6)} %select_n.2), kind=kOutput, calls=%fused_computation.9 | convolution fusion | flops 51249152 | bytes 1081604 | tf_op jit(solution)/shard_map/rs,rd->sd/dot_general | solution.py:432
  6.3 0.0 copy-done
  6.3 0.1 constant_dynamic-slice_fusion.1
  6.4 0.1 copy.51
  6.5 0.1 fusion.33
  6.6 0.7 fusion.34
  7.4 0.5 multiply_cosine_fusion
  7.9 0.1 subtract_convert_fusion.1
  8.0 1.0 fusion.24
  9.0 0.9 fusion.26
  9.9 0.0 copy-start.1
  9.9 0.7 pad_maximum_fusion.lat_ref
  10.7 50.4 %spread.1 = (bf16[2,2,8,24,2048]{4,3,2,1,0:T(8,128)(2,1)}, bf16[2,2,8,64,576]{4,3,2,1,0:T(8,128)(2,1)}) custom-call(bf16[8,24,2048]{2,1,0:T(8,128)(2,1)} %bitcast.51, bf16[64,576]{1,0:T(8,128)(2,1)} %pad_maximum_fusion.lat_ref), custom_call_target="tpu_custom_call" | custom-call | tf_op jit(solution)/shard_map/spread/pallas_call | solution.py:170
  61.1 0.0 copy-start.2
  61.1 3.5 %copy.42 = bf16[8,2,2,64,576]{4,3,2,1,0:T(8,128)(2,1)} copy(bf16[8,2,2,64,576]{4,3,0,1,2:T(8,128)(2,1)} %bitcast.52) | data formatting | bytes 4718592 | tf_op jit(solution)/shard_map/transpose | solution.py:438
  64.6 0.0 copy-done.1
  64.6 0.1 copy.43
  64.8 0.1 copy.44
  64.9 0.1 multiply_reduce_fusion
  65.0 0.0 copy-done.2
  65.0 0.1 multiply_multiply_fusion
  65.2 0.0 copy-start.6
  65.2 0.7 fusion.27.qn_ref
  65.8 0.2 subtract_convert_fusion
  66.0 0.8 maximum_bitcast_fusion.qr_ref
  66.8 4.9 %attend.1 = bf16[256,256]{1,0:T(8,128)(2,1)} custom-call(bf16[2048,576]{1,0:T(8,128)(2,1)} %bitcast.50, bf16[512,256]{1,0:T(8,128)(2,1)} %wk_ref.1, bf16[512,256]{1,0:T(8,128)(2,1)} %wv_ref.1, bf16[2,256,128]{2,1,0:T(8,128)(2,1)} %fusion.27.qn_ref, bf16[2,256,64]{2,1,0:T(8,128)(2,1)} %maximum_bitcast_fusion.qr_ref, f32[1,128]{1,0:T(1,128)} %bitcast.56, ...), custom_call_target="tpu_custom_call" | custom-call | tf_op jit(solution)/shard_map/attend/pallas_call | solution.py:356
  71.7 0.0 copy-done.6
  71.7 0.0 copy-start.4
  71.7 5.6 %fusion.2 = f32[2,2,8,24,896]{4,3,2,1,0:T(8,128)S(1)} fusion(bf16[2,2,8,24,2048]{4,3,2,1,0:T(8,128)(2,1)S(1)} %copy-done.6, bf16[1,2048,896]{2,1,0:T(8,128)(2,1)} %param.32), kind=kOutput, calls=%fused_computation.2 | convolution fusion | flops 2818572288 | bytes 9568256 | tf_op jit(solution)/shard_map/abecd,df->abecf/dot_general | solution.py:442
  77.4 0.0 copy-done.4
  77.4 0.0 copy-start.5
  77.4 3.8 %multiply_convert_fusion = bf16[2,2,8,24,896]{4,3,2,1,0:T(8,128)(2,1)S(1)} fusion(f32[2,2,8,24,896]{4,3,2,1,0:T(8,128)S(1)} %fusion.2, bf16[2,2,8,24,2048]{4,3,2,1,0:T(8,128)(2,1)S(1)} %copy-done.6, bf16[1,2048,896]{2,1,0:T(8,128)(2,1)S(1)} %copy-done.4), kind=kOutput, calls=%fused_computation.8 | convolution fusion | flops 2822701056 | bytes 10944512 | tf_op jit(solution)/shard_map/abecd,df->abecf/dot_general | solution.py:441
  81.1 0.0 copy-done.5
  81.1 4.8 %fusion.9.part_ref = bf16[2,8,2,24,2048]{4,3,2,1,0:T(8,128)(2,1)} fusion(bf16[1,896,2048]{2,1,0:T(8,128)(2,1)S(1)} %copy-done.5, bf16[2,2,8,24,896]{4,3,2,1,0:T(8,128)(2,1)S(1)} %multiply_convert_fusion), kind=kOutput, calls=%fused_computation.7 | convolution fusion | flops 2820145152 | bytes 8192000 | tf_op jit(solution)/shard_map/abecf,fd->aebcd/dot_general | solution.py:444
  86.0 37.3 %collect.1 = bf16[8,24,2048]{2,1,0:T(8,128)(2,1)} custom-call(bf16[2,8,2,24,2048]{4,3,2,1,0:T(8,128)(2,1)} %fusion.9.part_ref), custom_call_target="tpu_custom_call" | custom-call | tf_op jit(solution)/shard_map/collect/pallas_call | solution.py:277
  123.3 0.0 copy-done.3
  123.3 0.1 constant_dynamic-slice_fusion
  123.3 2.3 %fusion.15 = bf16[64,2048]{1,0:T(8,128)(2,1)} fusion(bf16[192,2048,1]{1,0,2:T(8,128)(2,1)} %bitcast.55, f32[64,2]{0,1:T(2,128)S(1)} %constant_dynamic-slice_fusion, s32[64,2]{0,1:T(2,128)S(1)} %multiply_add_fusion), kind=kOutput, calls=%fused_computation.12 | convolution fusion | flops 101081088 | bytes 1049600 | tf_op jit(solution)/shard_map/rks,sd->rkd/dot_general | solution.py:464
  (8 shorter events, 0.0 us)
Async XLA Ops:
  0.6 5.7 %copy-start = (bf16[256,64]{0,1:T(8,128)(2,1)S(1)}, bf16[256,64]{0,1:T(8,128)(2,1)}, u32[]{:S(2)}) copy-start(bf16[256,64]{0,1:T(8,128)(2,1)} %param.19) | copy-start | bytes 98308
  9.9 54.7 %copy-start.1 = (bf16[256,384]{1,0:T(8,128)(2,1)S(1)}, bf16[256,384]{1,0:T(8,128)(2,1)}, u32[]{:S(2)}) copy-start(bf16[256,384]{1,0:T(8,128)(2,1)} %param.17) | copy-start | bytes 589828
  61.1 3.9 %copy-start.2 = (f32[192]{0:T(256)S(1)}, f32[192]{0:T(256)}, u32[]{:S(2)}) copy-start(f32[192]{0:T(256)} %param.23) | copy-start | bytes 2308
  65.2 6.5 %copy-start.6 = (bf16[2,2,8,24,2048]{4,3,2,1,0:T(8,128)(2,1)S(1)}, bf16[2,2,8,24,2048]{4,3,2,1,0:T(8,128)(2,1)}, u32[]{:S(2)}) copy-start(bf16[2,2,8,24,2048]{4,3,2,1,0:T(8,128)(2,1)} %get-tuple-element.5) | copy-start | bytes 9437188
  71.7 5.6 %copy-start.4 = (bf16[1,2048,896]{2,1,0:T(8,128)(2,1)S(1)}, bf16[1,2048,896]{2,1,0:T(8,128)(2,1)}, u32[]{:S(2)}) copy-start(bf16[1,2048,896]{2,1,0:T(8,128)(2,1)} %param.31) | copy-start | bytes 11010052
  77.4 3.8 %copy-start.5 = (bf16[1,896,2048]{2,1,0:T(8,128)(2,1)S(1)}, bf16[1,896,2048]{2,1,0:T(8,128)(2,1)}, u32[]{:S(2)}) copy-start(bf16[1,896,2048]{2,1,0:T(8,128)(2,1)} %param.33) | copy-start | bytes 11010052
  86.0 37.3 %copy-start.3 = (f32[256,2]{0,1:T(2,128)S(1)}, f32[256,2]{0,1:T(2,128)}, u32[]{:S(2)}) copy-start(f32[256,2]{0,1:T(2,128)} %param.30) | copy-start | bytes 6148
where the time goes:
time: 126 us
  Pallas kernels  92.6 us (73%)
  matrix products  18.9 us (15%)
  other arithmetic  7.22 us (6%)
  local copies, waits for them, and re-layouts  5.99 us (5%)
    pallas_call x1, Pallas kernels, spread(): pl.pallas_call(functools.partial(spread_kernel, n_ep, highs), out_shape=(...  50.4 us
    pallas_call x1, Pallas kernels, collect(): pl.pallas_call(functools.partial(collect_kernel, n_ep, highs), out_shape=...  37.3 us
    dot_general x1, matrix products, on_device(): jnp.einsum('abecd,df->abecf', arrived, w_up[0], preferred_element_type=jn...  5.64 us
    pallas_call x1, Pallas kernels, attend(): pl.pallas_call(functools.partial(attend_kernel, heads, nope_dim, value_di...  4.94 us
    dot_general x1, matrix products, on_device(): jnp.einsum('abecf,fd->aebcd', hidden, w_down[0], preferred_element_type=j...  4.82 us
    dot_general x1, matrix products, on_device(): jnp.einsum('abecd,df->abecf', arrived, w_gate[0], preferred_element_type=...  3.75 us
    transpose x1, local copies, waits for them, and re-layouts, on_device(): jnp.transpose(lat_all, (2, 1, 0, 3, 4))  3.54 us

commit v1 on v0

--- a/solution.py
+++ b/solution.py
@@ -369,6 +369,451 @@
     )(
         lat_rows, w_key_up, w_value_up, query_nope, query_rope,
         key_gain.reshape(1, -1), out_gain.reshape(1, -1),
+    )
+
+
+LANES = 128
+TILE = 256
+
+
+def layer_kernel(
+    n_ep, heads, nope_dim, rope_dim, value_dim,
+    q_ref, kv_ref, rk_ref, cos_ref, sin_ref, lg_ref, wk_ref, wv_ref, qg_ref, kg_ref, rg_ref, og_ref,
+    tok_ref, mg_ref, routes_ref, rw_ref, wg_hbm, wu_hbm, wd_hbm,
+    att_ref, moe_ref,
+    wgu, wd, rows_out, arrived, hid, part, low_buf, sum_buf, high_buf, final_buf, ret, hits,
+    lat_all, qn, qr, acc, den,
+    w_sem, ep_send, ep_recv, high_send, high_recv, low_send, low_recv,
+    rlow_send, rlow_recv, rhigh_send, rhigh_recv, rep_send, rep_recv,
+    lz_send, lz_recv, ly_send, ly_recv, ll_send, ll_recv,
+):
+    me, quarter = lax.axis_index("ep"), lax.axis_index("tp")
+    n_z = n_ep // 2
+    z, y = me // 2, lax.rem(me, 2)
+    high, low = quarter // 2, lax.rem(quarter, 2)
+    partner = (me, high * 2 + 1 - low)
+    across = (me, (1 - high) * 2 + low)
+    bf16, f32 = jnp.bfloat16, jnp.float32
+    cap = rows_out.shape[1]
+    model_dim = rows_out.shape[2]
+    tok_rows = tok_ref.shape[0]
+    part_rows = tok_rows // 4
+    ff = wd.shape[0]
+    barrier = pltpu.get_barrier_semaphore()
+
+    def hello(device):
+        pl.semaphore_signal(barrier, inc=1, device_id=device, device_id_type=MESH)
+
+    def hello_ep(step, carry):
+        hello((lax.rem(me + step, n_ep), quarter))
+        return carry
+
+    lax.fori_loop(1, n_ep, hello_ep, 0)
+    hello(partner)
+    hello(across)
+
+    def weight_copies():
+        out = []
+        for i in range(ff // LANES):
+            out.append((wg_hbm.at[0, :, pl.ds(LANES * i, LANES)], wgu.at[:, pl.ds(TILE * i, LANES)]))
+            out.append((wu_hbm.at[0, :, pl.ds(LANES * i, LANES)], wgu.at[:, pl.ds(TILE * i + LANES, LANES)]))
+        out.append((wd_hbm.at[0], wd))
+        return [pltpu.make_async_copy(a, b, w_sem.at[i]) for i, (a, b) in enumerate(out)]
+
+    for copy in weight_copies():
+        copy.start()
+
+    def ep_to(s, t):
+        return lax.rem(z + s, n_z) * 2 + lax.rem(y + t, 2)
+
+    def ep_from(s, t):
+        return lax.rem(z + n_z - s, n_z) * 2 + lax.rem(y + t, 2)
+
+
+    def normed_rows(q):
+        rows = tok_ref[pl.ds(pl.multiple_of(q * part_rows, part_rows), part_rows), :].astype(f32)
+        return rms_norm(rows, mg_ref[...]).astype(bf16)
+
+    def earlier_matrix():
+        shape = (part_rows, part_rows)
+        return (lax.broadcasted_iota(jnp.int32, shape, 0) > lax.broadcasted_iota(jnp.int32, shape, 1)).astype(bf16)
+
+    def own_routes(q):
+        return routes_ref[pl.ds(pl.multiple_of(q * part_rows, part_rows), part_rows), :]
+
+    def dispatch():
+        chosen = own_routes(quarter)
+        experts = lax.broadcasted_iota(jnp.int32, (part_rows, LANES), 1)
+        ones = [(chosen[:, k : k + 1] == experts).astype(f32) for k in range(2)]
+        rank = jnp.dot(earlier_matrix(), (ones[0] + ones[1]).astype(bf16), preferred_element_type=f32)
+        slot_ids = lax.broadcasted_iota(jnp.int32, (part_rows, n_ep * cap), 1).astype(f32)
+        for k in range(2):
+            own_rank = jnp.sum(rank * ones[k], axis=-1, keepdims=True)
+            slot = chosen[:, k : k + 1].astype(f32) * cap + own_rank
+            hits[k] = (slot_ids == slot).astype(bf16)
+        select = (hits[0].astype(f32) + hits[1].astype(f32)).astype(bf16)
+        rows = normed_rows(quarter)
+        wide = 512
+        for n in range(model_dim // wide):
+            picked = lax.dot_general(
+                select, rows[:, n * wide : (n + 1) * wide], (((0,), (0,)), ((), ())), preferred_element_type=f32
+            )
+            rows_out[:, :, n * wide : (n + 1) * wide] = picked.astype(bf16).reshape(n_ep, cap, wide)
+
+    def own_dispatch(q, carry):
+        chosen = own_routes(q)
+        names = jnp.sum((chosen == me).astype(f32), axis=-1, keepdims=True)
+        named = jnp.broadcast_to(names, (part_rows, LANES))
+        rank = jnp.dot(earlier_matrix(), named.astype(bf16), preferred_element_type=f32)
+        slot_ids = lax.broadcasted_iota(jnp.int32, (part_rows, LANES), 1).astype(f32)
+        select = jnp.where(slot_ids == rank, named, 0.0).astype(bf16)[:, :cap]
+        picked = lax.dot_general(
+            select, normed_rows(q), (((0,), (0,)), ((), ())), preferred_element_type=f32
+        )
+        arrived[me, lax.rem(q, 2), q // 2] = picked.astype(bf16)
+        return carry
+
+    dispatch()
+    pl.semaphore_wait(barrier, n_ep + 1)
+
+    def ep_copy(s, t):
+        return remote(
+            rows_out.at[ep_to(s, t)], arrived.at[me, low, high], ep_send.at[s, t], ep_recv.at[s, t],
+            (ep_to(s, t), quarter),
+        )
+
+    def ep_arrival(s, t):
+        j = ep_from(s, t)
+        return remote(
+            rows_out.at[j], arrived.at[j, low, high], ep_send.at[s, t], ep_recv.at[s, t], (j, quarter)
+        )
+
+    def high_copy(s, t, side):
+        block = arrived.at[ep_from(s, t), low, side]
+        return remote(block, block, high_send.at[s, t], high_recv.at[s, t], across)
+
+    def low_copy(s, t, hop, side, core):
+        block = arrived.at[ep_from(s, t), core, side]
+        return remote(block, block, low_send.at[hop, s, t], low_recv.at[hop, s, t], partner)
+
+    def each(s, body):
+        for t in range(2):
+            if t == 0:
+                pl.when(s > 0)(functools.partial(body, s, 0))
+            else:
+                body(s, 1)
+
+    def start_ep(s, carry):
+        each(s, lambda s, t: ep_copy(s, t).start())
+        return carry
+
+    lax.fori_loop(1, n_z, start_ep, 0)
+    start_ep(0, 0)
+
+
+    def lat_copy_z(k):
+        block = lat_all.at[k, y, low]
+        return remote(
+            block, block, lz_send.at[k], lz_recv.at[k], (lax.rem(z + 1, n_z) * 2 + y, quarter)
+        )
+
+    def lat_copy_y(k, side):
+        block = lat_all.at[k, side, low]
+        return remote(block, block, ly_send.at[k], ly_recv.at[k], (z * 2 + 1 - y, quarter))
+
+    def lat_copy_low(k, hop, core):
+        block = lat_all.at[k, y if hop == 0 else 1 - y, core]
+        return remote(block, block, ll_send.at[hop, k], ll_recv.at[hop, k], partner)
+
+    def lat_own():
+        latent = rms_norm(kv_ref[...].astype(f32), lg_ref[...]).astype(bf16)
+        rot = rotate(rms_norm(rk_ref[...].astype(f32), rg_ref[...]), cos_ref[...], sin_ref[...]).astype(bf16)
+        half = tok_rows // 2
+        width = latent.shape[1]
+        for core in range(2):
+            lat_all[z, y, core, :, :width] = latent[core * half : (core + 1) * half]
+            lat_all[z, y, core, :, width:] = rot[core * half : (core + 1) * half]
+        pl.when(z < n_z - 1)(lambda: lat_copy_z(z).start())
+        pl.when(y == 0)(lambda: lat_copy_y(z, y).start())
+
+    def lat_step(k, carry):
+        origin = z - k
+
+        @pl.when(origin >= 0)
+        def _():
+            lat_copy_z(origin).wait_recv()
+            pl.when(z < n_z - 1)(lambda: lat_copy_z(origin).start())
+            lat_copy_y(origin, y).start()
+            lat_copy_low(origin, 0, low).start()
+
+        return carry
+
+    def lat_side(k, carry):
+        origin = z - k
+
+        @pl.when((origin >= 0) & (k + y > 0))
+        def _():
+            lat_copy_y(origin, 1 - y).wait_recv()
+            lat_copy_low(origin, 1, low).start()
+
+        return carry
+
+
+    def queries():
+        raw = q_ref[...].astype(f32)
+        width = nope_dim + rope_dim
+        for head in range(heads):
+            query = rms_norm(raw[:, head * width : (head + 1) * width], qg_ref[...])
+            qn[head] = query[:, :nope_dim].astype(bf16)
+            qr[head] = rotate(query[:, nope_dim:], cos_ref[...], sin_ref[...]).astype(bf16)
+
+    scale = (nope_dim + rope_dim) ** (-0.5)
+
+    def attend_block(zj, yj, own):
+        block = lat_all[zj, yj].reshape(tok_rows, lat_all.shape[-1])
+        width = block.shape[1] - rope_dim
+        latent, rot_key = block[:, :width], block[:, width:]
+        keys = jnp.dot(latent, wk_ref[...], preferred_element_type=f32)
+        values = jnp.dot(latent, wv_ref[...], preferred_element_type=f32).astype(bf16)
+        lined = (((1,), (1,)), ((), ()))
+        for head in range(heads):
+            key = rms_norm(keys[:, head * nope_dim : (head + 1) * nope_dim], kg_ref[...]).astype(bf16)
+            scores = lax.dot_general(qn[head], key, lined, preferred_element_type=f32)
+            scores = scores + lax.dot_general(qr[head], rot_key, lined, preferred_element_type=f32)
+            weights = jnp.exp(scores * scale)
+            if own:
+                shape = (tok_rows, tok_rows)
+                visible = lax.broadcasted_iota(jnp.int32, shape, 0) >= lax.broadcasted_iota(jnp.int32, shape, 1)
+                weights = jnp.where(visible, weights, 0.0)
+            total = jnp.sum(weights, axis=-1, keepdims=True)
+            mixed = jnp.dot(
+                weights.astype(bf16), values[:, head * value_dim : (head + 1) * value_dim],
+                preferred_element_type=f32,
+            )
+            if own:
+                den[head] = total
+                acc[head] = mixed
+            else:
+                den[head] += total
+                acc[head] += mixed
+
+    def attend_side(k):
+        @pl.when((z >= k) & (k + y > 0))
+        def _():
+            lat_copy_low(z - k, 1, 1 - low).wait_recv()
+            attend_block(z - k, 1 - y, False)
+
+    def attend_line(k):
+        @pl.when(z >= k)
+        def _():
+            lat_copy_low(z - k, 0, 1 - low).wait_recv()
+            attend_block(z - k, y, False)
+
+
+    def forward(s, t):
+        ep_arrival(s, t).wait_recv()
+        high_copy(s, t, high).start()
+        low_copy(s, t, 0, high, low).start()
+
+    def forward_low(s, t):
+        high_copy(s, t, 1 - high).wait_recv()
+        low_copy(s, t, 1, 1 - high, low).start()
+
+    def arrive(s, t):
+        low_copy(s, t, 0, high, 1 - low).wait_recv()
+        low_copy(s, t, 1, 1 - high, 1 - low).wait_recv()
+
+    def expert(s):
+        first = lax.rem(z + n_z - s, n_z) * 2
+        rows = arrived[pl.ds(first, 2)].reshape(8 * cap, model_dim)
+        for i in range(ff // LANES):
+            both = jnp.dot(rows, wgu[:, TILE * i : TILE * (i + 1)], preferred_element_type=f32)
+            gate, upward = both[:, :LANES], both[:, LANES:]
+            hid[:, LANES * i : LANES * (i + 1)] = (jax.nn.silu(gate) * upward).astype(bf16)
+        for n in range(model_dim // TILE):
+            down = jnp.dot(hid[...], wd[:, TILE * n : TILE * (n + 1)], preferred_element_type=f32)
+            part[pl.ds(first, 2), :, :, :, TILE * n : TILE * (n + 1)] = down.astype(bf16).reshape(
+                2, 2, 2, cap, TILE
+            )
+
+    def rlow_copy(s, t):
+        j = ep_from(s, t)
+        return remote(part.at[j, 1 - low], low_buf.at[j], rlow_send.at[s, t], rlow_recv.at[s, t], partner)
+
+    def rhigh_copy(s, t):
+        j = ep_from(s, t)
+        return remote(sum_buf.at[j], high_buf.at[j], rhigh_send.at[s, t], rhigh_recv.at[s, t], across)
+
+    def rep_copy(s, t):
+        j = ep_from(s, t)
+        return remote(final_buf.at[j], ret.at[me], rep_send.at[s, t], rep_recv.at[s, t], (j, quarter))
+
+    def rep_arrival(s, t):
+        j = ep_to(s, t)
+        return remote(final_buf.at[j], ret.at[j], rep_send.at[s, t], rep_recv.at[s, t], (j, quarter))
+
+    def reduce_low(s):
+        for t in range(2):
+            j = ep_from(s, t)
+            rlow_copy(s, t).wait_recv()
+            sum_buf[j] = (part[j, low, 1 - high].astype(f32) + low_buf[j, 1 - high].astype(f32)).astype(bf16)
+            rhigh_copy(s, t).start()
+
+    def reduce_high(s):
+        for t in range(2):
+            j = ep_from(s, t)
+            rhigh_copy(s, t).wait_recv()
+            value = part[j, low, high].astype(f32) + low_buf[j, high].astype(f32) + high_buf[j].astype(f32)
+            value = value.astype(bf16)
+            if t == 0:
+
+                @pl.when(s == 0)
+                def _():
+                    ret[me] = value
+
+                @pl.when(s > 0)
+                def _():
+                    final_buf[j] = value
+                    rep_copy(s, 0).start()
+            else:
+                final_buf[j] = value
+                rep_copy(s, 1).start()
+
+    lax.fori_loop(0, 4, own_dispatch, 0)
+    lat_own()
+    queries()
+    attend_block(z, y, True)
+
+    def stage(s, carry):
+        each(s, forward)
+        each(s, forward_low)
+        each(s, arrive)
+
+        @pl.when(s == 0)
+        def _():
+            for copy in weight_copies():
+                copy.wait()
+
+        expert(s)
+        for t in range(2):
+            rlow_copy(s, t).start()
+        pl.when(s > 0)(lambda: reduce_low(s - 1))
+        pl.when(s > 1)(lambda: reduce_high(s - 2))
+        return carry
+
+    lax.fori_loop(0, n_z, stage, 0)
+    lax.fori_loop(1, n_z, lat_step, 0)
+    reduce_low(n_z - 1)
+    reduce_high(n_z - 2)
+    lax.fori_loop(0, n_z, lat_side, 0)
+    reduce_high(n_z - 1)
+
+    def attend_step(k, carry):
+        pl.when(k > 0)(lambda: attend_line(k))
+        attend_side(k)
+        return carry
+
+    lax.fori_loop(0, n_z, attend_step, 0)
+    for head in range(heads):
+        mixed = rms_norm(acc[head] / den[head], og_ref[...])
+        att_ref[:, head * value_dim : (head + 1) * value_dim] = mixed.astype(bf16)
+
+    def returned(s, carry):
+        each(s, lambda s, t: rep_arrival(s, t).wait_recv())
+        return carry
+
+    lax.fori_loop(0, n_z, returned, 0)
+    weights = rw_ref[pl.ds(pl.multiple_of(quarter * part_rows, part_rows), part_rows), :]
+    wide = 512
+    for n in range(model_dim // wide):
+        values = ret[:, :, n * wide : (n + 1) * wide].reshape(n_ep * cap, wide)
+        mixed = jnp.dot(hits[0], values, preferred_element_type=f32) * weights[:, 0:1]
+        mixed += jnp.dot(hits[1], values, preferred_element_type=f32) * weights[:, 1:2]
+        moe_ref[:, n * wide : (n + 1) * wide] = mixed.astype(bf16)
+
+    def sent(s, carry):
+        def rows_sent(s, t):
+            ep_copy(s, t).wait_send()
+            high_copy(s, t, high).wait_send()
+            low_copy(s, t, 0, high, low).wait_send()
+            low_copy(s, t, 1, 1 - high, low).wait_send()
+            rep_copy(s, t).wait_send()
+
+        each(s, rows_sent)
+        for t in range(2):
+            rlow_copy(s, t).wait_send()
+            rhigh_copy(s, t).wait_send()
+
+        origin = z - s
+
+        @pl.when(origin >= 0)
+        def _():
+            pl.when(z < n_z - 1)(lambda: lat_copy_z(origin).wait_send())
+            pl.when((s > 0) | (y == 0))(lambda: lat_copy_y(origin, y).wait_send())
+            pl.when(s > 0)(lambda: lat_copy_low(origin, 0, low).wait_send())
+            pl.when(s + y > 0)(lambda: lat_copy_low(origin, 1, low).wait_send())
+
+        return carry
+
+    lax.fori_loop(0, n_z, sent, 0)
+
+
+def layer(
+    queries, kv_latent, rope_key, rot_cos, rot_sin, latent_gain, w_key_up, w_value_up, query_gain, key_gain,
+    rope_gain, out_gain, moe_tokens, moe_gain, routes, route_weights, w_gate, w_up, w_down, n_ep, cap,
+):
+    tok_rows = queries.shape[0]
+    nope_dim, rope_dim, value_dim = key_gain.shape[0], rope_key.shape[1], out_gain.shape[0]
+    heads = w_key_up.shape[1] // nope_dim
+    model_dim = moe_tokens.shape[1]
+    part_rows = tok_rows // 4
+    ff = w_down.shape[1]
+    n_z = n_ep // 2
+    width = kv_latent.shape[1] + rope_dim
+    dma = pltpu.SemaphoreType.DMA
+    kind = jnp.bfloat16
+    pairs = (n_z, 2)
+    block = (cap, model_dim)
+    vmem, anywhere = pl.BlockSpec(memory_space=VMEM), pl.BlockSpec(memory_space=pl.ANY)
+    return pl.pallas_call(
+        functools.partial(layer_kernel, n_ep, heads, nope_dim, rope_dim, value_dim),
+        out_shape=(
+            jax.ShapeDtypeStruct((tok_rows, heads * value_dim), kind),
+            jax.ShapeDtypeStruct((part_rows, model_dim), kind),
+        ),
+        in_specs=[vmem] * 16 + [anywhere] * 3,
+        out_specs=(vmem, vmem),
+        scratch_shapes=[
+            VMEM((model_dim, 2 * ff), kind),
+            VMEM((ff, model_dim), kind),
+            VMEM((n_ep,) + block, kind),
+            VMEM((n_ep, 2, 2) + block, kind),
+            VMEM((8 * cap, ff), kind),
+            VMEM((n_ep, 2, 2) + block, kind),
+            VMEM((n_ep, 2) + block, kind),
+            VMEM((n_ep,) + block, kind),
+            VMEM((n_ep,) + block, kind),
+            VMEM((n_ep,) + block, kind),
+            VMEM((n_ep,) + block, kind),
+            VMEM((2, part_rows, n_ep * cap), kind),
+            VMEM((n_z, 2, 2, tok_rows // 2, width), kind),
+            VMEM((heads, tok_rows, nope_dim), kind),
+            VMEM((heads, tok_rows, rope_dim), kind),
+            VMEM((heads, tok_rows, value_dim), jnp.float32),
+            VMEM((heads, tok_rows, 1), jnp.float32),
+            dma((2 * (ff // LANES) + 1,)),
+            dma(pairs), dma(pairs), dma(pairs), dma(pairs), dma((2,) + pairs), dma((2,) + pairs),
+            dma(pairs), dma(pairs), dma(pairs), dma(pairs), dma(pairs), dma(pairs),
+            dma((n_z,)), dma((n_z,)), dma((n_z,)), dma((n_z,)), dma((2, n_z)), dma((2, n_z)),
+        ],
+        compiler_params=pltpu.CompilerParams(
+            collective_id=2, has_side_effects=True, vmem_limit_bytes=62 << 20
+        ),
+        name="layer",
+    )(
+        queries, kv_latent, rope_key, rot_cos, rot_sin, latent_gain.reshape(1, -1), w_key_up, w_value_up,
+        query_gain.reshape(1, -1), key_gain.reshape(1, -1), rope_gain.reshape(1, -1), out_gain.reshape(1, -1),
+        moe_tokens, moe_gain.reshape(1, -1), routes, route_weights, w_gate, w_up, w_down,
     )
 
 
@@ -401,6 +846,18 @@
     head_count = w_key_up.shape[1] // nope_dim
     positions = lax.axis_index("ep") * tok_rows + jnp.arange(tok_rows, dtype=jnp.int32)
     rot_cos, rot_sin = rope_tables(positions, rope_dim)
+    n_rows, model_dim = moe_tokens.shape
+    top_count = routes.shape[1]
+    part_rows = n_rows // quarters
+    experts = n_ep * w_gate.shape[0]
+    capacity = (3 * top_count * part_rows + 2 * experts - 1) // (2 * experts)
+    one_kernel = quarters == 4 and n_ep % 2 == 0 and w_gate.shape[0] == 1 and top_count == 2
+    if one_kernel and capacity % 8 == 0 and w_down.shape[1] % LANES == 0 and model_dim % 512 == 0:
+        return layer(
+            queries, kv_latent, rope_key, rot_cos, rot_sin, latent_gain, w_key_up, w_value_up, query_gain,
+            key_gain, rope_gain, out_gain, moe_tokens, moe_gain, routes, route_weights, w_gate, w_up, w_down,
+            n_ep, capacity,
+        )
     lat_part = tok_rows // quarters
 
     def mine(values, rows):
@@ -414,11 +871,6 @@
     )
     lat_own = jnp.concatenate([latent.astype(jnp.bfloat16), rot_key.astype(jnp.bfloat16)], axis=1)
 
-    n_rows, model_dim = moe_tokens.shape
-    top_count = routes.shape[1]
-    part_rows = n_rows // quarters
-    experts = n_ep * w_gate.shape[0]
-    capacity = (3 * top_count * part_rows + 2 * experts - 1) // (2 * experts)
     slot_count = experts * capacity
     own_rows = rms_norm(mine(moe_tokens, part_rows).astype(jnp.float32), moe_gain).astype(jnp.bfloat16)
     chosen = mine(routes, part_rows).reshape(part_rows * top_count)

time: 126 us -> 105 us (0.83)
  matrix products: 18.9 us -> 0 us
  other arithmetic: 7.22 us -> 1.25 us
  Pallas kernels: 92.6 us -> 94.8 us
  local copies, waits for them, and re-layouts: 5.99 us -> 7.66 us
    dot_general x6 -> x0, matrix products: 18.9 us -> none  [the longest x1 5.64 us: on_device(): jnp.einsum('abecd,df->abecf', arrived, w_up[0], preferred_element_type=jn...]
    unnamed x16 -> x5, local copies, waits for them, and re-layouts: 0.28 us -> 7.66 us
    transpose x2 -> x0, local copies, waits for them, and re-layouts: 4.21 us -> none  [the longest x1 3.54 us: on_device(): jnp.transpose(lat_all, (2, 1, 0, 3, 4))]
    reduce_sum x5 -> x0, other arithmetic: 2.33 us -> none  [the longest x4 2.24 us: rms_norm(): jnp.mean(values * values, axis=-1, keepdims=True) + EPS]
    pallas_call x3 -> x1, Pallas kernels: 92.6 us -> 94.8 us  [layer(): pl.pallas_call(functools.partial(layer_kernel, n_ep, heads, nope_dim, rop...]
where the time goes in v1:
time: 105 us; the launch traced here: 104 us
  Pallas kernels  94.8 us (90%)
  local copies, waits for them, and re-layouts  7.66 us (7%)
  other arithmetic  1.25 us (1%)
    pallas_call x1, Pallas kernels, layer(): pl.pallas_call(functools.partial(layer_kernel, n_ep, heads, nope_dim, rop...  94.8 us
    unnamed x5, local copies, waits for them, and re-layouts  7.66 us

profile of v1, /device:TPU:0, one launch (start us, length us, event | category | flops | bytes accessed | tf_op | source)
XLA Modules:
  0.0 104.3 jit_solution(17467250102801878793)
XLA Ops:
  0.7 1.5 %copy.23.rk_ref = bf16[256,64]{1,0:T(8,128)(2,1)} copy(bf16[256,64]{0,1:T(8,128)(2,1)} %param.19) | data formatting | bytes 65536 | tf_op args[2]
  2.1 1.5 %copy.24.routes_ref = s32[256,2]{1,0:T(8,128)} copy(s32[256,2]{0,1:T(2,128)} %param.29) | data formatting | bytes 4096 | tf_op args[12]
  3.6 1.5 %copy.25.rw_ref = f32[256,2]{1,0:T(8,128)} copy(f32[256,2]{0,1:T(2,128)} %param.30) | data formatting | bytes 4096 | tf_op args[13]
  5.1 1.2 %multiply_sine_fusion = (f32[256,32]{1,0:T(8,128)}, f32[256,32]{1,0:T(8,128)}) fusion(f32[256]{0:T(256)S(1)} %add_convert_fusion, f32[32]{0:T(128)S(1)} %negate_power_fusion), kind=kLoop, calls=%fused_computation | loop fusion | flops 8192 | bytes 66688 | tf_op jit(solution)/shard_map/sin | solution.py:22
  6.3 94.8 %layer.1 = (bf16[256,256]{1,0:T(8,128)(2,1)}, bf16[64,2048]{1,0:T(8,128)(2,1)}) custom-call(bf16[256,384]{1,0:T(8,128)(2,1)} %q_ref.1, bf16[256,512]{1,0:T(8,128)(2,1)} %kv_ref.1, bf16[256,64]{1,0:T(8,128)(2,1)} %copy.23.rk_ref, f32[256,32]{1,0:T(8,128)} %get-tuple-element.3.cos_ref, f32[256,32]{1,0:T(8,128)} %get-tuple-element.2.sin_ref, f32[1,512]{1,0:T(1,128)} %bitcast.7, ...), custom_call_target="tpu_custom_call" | custom-call | tf_op jit(solution)/shard_map/layer/pallas_call | solution.py:778
  101.1 1.6 %copy.28 = bf16[256,256]{1,0:T(8,128)(2,1)} copy(bf16[256,256]{1,0:T(8,128)(2,1)} %get-tuple-element.6) | data formatting | bytes 262144
  102.7 1.7 %copy.29 = bf16[64,2048]{1,0:T(8,128)(2,1)} copy(bf16[64,2048]{1,0:T(8,128)(2,1)} %get-tuple-element.7) | data formatting | bytes 524288
  (2 shorter events, 0.0 us)

commit v2 on v1

--- a/solution.py
+++ b/solution.py
@@ -378,12 +378,14 @@
 
 def layer_kernel(
     n_ep, heads, nope_dim, rope_dim, value_dim,
-    q_ref, kv_ref, rk_ref, cos_ref, sin_ref, lg_ref, wk_ref, wv_ref, qg_ref, kg_ref, rg_ref, og_ref,
-    tok_ref, mg_ref, routes_ref, rw_ref, wg_hbm, wu_hbm, wd_hbm,
+    tok_hbm, mg_hbm, routes_hbm, rw_hbm, kv_hbm, rk_hbm, freq_hbm, lg_hbm, rg_hbm, q_hbm, qg_hbm,
+    wk_hbm, wv_hbm, kg_hbm, og_hbm, wg_hbm, wu_hbm, wd_hbm,
     att_ref, moe_ref,
-    wgu, wd, rows_out, arrived, hid, part, low_buf, sum_buf, high_buf, final_buf, ret, hits,
-    lat_all, qn, qr, acc, den,
-    w_sem, ep_send, ep_recv, high_send, high_recv, low_send, low_recv,
+    tok_ref, mg_ref, routes_ref, rw_ref, kv_ref, rk_ref, freq_ref, lg_ref, rg_ref, q_ref, qg_ref,
+    wk_ref, wv_ref, kg_ref, og_ref,
+    wgu, wd, normed, rows_out, arrived, hid, part, low_buf, sum_buf, high_buf, final_buf, ret, hits,
+    lat_all, cos_ref, sin_ref, qn, qr, acc, den,
+    in_sem, w_sem, ep_send, ep_recv, high_send, high_recv, low_send, low_recv,
     rlow_send, rlow_recv, rhigh_send, rhigh_recv, rep_send, rep_recv,
     lz_send, lz_recv, ly_send, ly_recv, ll_send, ll_recv,
 ):
@@ -420,6 +422,20 @@
         out.append((wd_hbm.at[0], wd))
         return [pltpu.make_async_copy(a, b, w_sem.at[i]) for i, (a, b) in enumerate(out)]
 
+    sources = (
+        tok_hbm, mg_hbm, routes_hbm, rw_hbm, kv_hbm, rk_hbm, freq_hbm, lg_hbm, rg_hbm, q_hbm, qg_hbm,
+        wk_hbm, wv_hbm, kg_hbm, og_hbm,
+    )
+    loaded = (
+        tok_ref, mg_ref, routes_ref, rw_ref, kv_ref, rk_ref, freq_ref, lg_ref, rg_ref, q_ref, qg_ref,
+        wk_ref, wv_ref, kg_ref, og_ref,
+    )
+    loads = [
+        pltpu.make_async_copy(source, into, in_sem.at[i])
+        for i, (source, into) in enumerate(zip(sources, loaded))
+    ]
+    for copy in loads:
+        copy.start()
     for copy in weight_copies():
         copy.start()
 
@@ -430,50 +446,83 @@
         return lax.rem(z + n_z - s, n_z) * 2 + lax.rem(y + t, 2)
 
 
-    def normed_rows(q):
-        rows = tok_ref[pl.ds(pl.multiple_of(q * part_rows, part_rows), part_rows), :].astype(f32)
-        return rms_norm(rows, mg_ref[...]).astype(bf16)
-
-    def earlier_matrix():
-        shape = (part_rows, part_rows)
-        return (lax.broadcasted_iota(jnp.int32, shape, 0) > lax.broadcasted_iota(jnp.int32, shape, 1)).astype(bf16)
-
-    def own_routes(q):
-        return routes_ref[pl.ds(pl.multiple_of(q * part_rows, part_rows), part_rows), :]
-
-    def dispatch():
-        chosen = own_routes(quarter)
-        experts = lax.broadcasted_iota(jnp.int32, (part_rows, LANES), 1)
-        ones = [(chosen[:, k : k + 1] == experts).astype(f32) for k in range(2)]
-        rank = jnp.dot(earlier_matrix(), (ones[0] + ones[1]).astype(bf16), preferred_element_type=f32)
-        slot_ids = lax.broadcasted_iota(jnp.int32, (part_rows, n_ep * cap), 1).astype(f32)
-        for k in range(2):
-            own_rank = jnp.sum(rank * ones[k], axis=-1, keepdims=True)
-            slot = chosen[:, k : k + 1].astype(f32) * cap + own_rank
-            hits[k] = (slot_ids == slot).astype(bf16)
-        select = (hits[0].astype(f32) + hits[1].astype(f32)).astype(bf16)
-        rows = normed_rows(quarter)
+    tokens = (1, tok_rows)
+    token = lax.broadcasted_iota(jnp.int32, tokens, 1)
+
+    def quarter_of(index):
+        return sum((index >= q * part_rows).astype(jnp.int32) for q in range(1, 4))
+
+    def hit_matrix(count, places):
+        slot = lax.broadcasted_iota(jnp.int32, (count, places[0].shape[1]), 0).astype(f32)
+        return sum((slot == place).astype(f32) for place in places)
+
+    def gather_rows(select, into):
+        select = select.astype(bf16)
         wide = 512
         for n in range(model_dim // wide):
-            picked = lax.dot_general(
-                select, rows[:, n * wide : (n + 1) * wide], (((0,), (0,)), ((), ())), preferred_element_type=f32
-            )
-            rows_out[:, :, n * wide : (n + 1) * wide] = picked.astype(bf16).reshape(n_ep, cap, wide)
-
-    def own_dispatch(q, carry):
-        chosen = own_routes(q)
-        names = jnp.sum((chosen == me).astype(f32), axis=-1, keepdims=True)
-        named = jnp.broadcast_to(names, (part_rows, LANES))
-        rank = jnp.dot(earlier_matrix(), named.astype(bf16), preferred_element_type=f32)
-        slot_ids = lax.broadcasted_iota(jnp.int32, (part_rows, LANES), 1).astype(f32)
-        select = jnp.where(slot_ids == rank, named, 0.0).astype(bf16)[:, :cap]
-        picked = lax.dot_general(
-            select, normed_rows(q), (((0,), (0,)), ((), ())), preferred_element_type=f32
-        )
-        arrived[me, lax.rem(q, 2), q // 2] = picked.astype(bf16)
-        return carry
-
-    dispatch()
+            cols = slice(n * wide, (n + 1) * wide)
+            rows = jnp.dot(select, normed[:, cols], preferred_element_type=f32).astype(bf16)
+            into(cols, rows, wide)
+
+    def own_part(row):
+        return sum(
+            jnp.where(quarter == q, row[:, q * part_rows : (q + 1) * part_rows], 0.0) for q in range(4)
+        )
+
+    def ranks():
+        shape = (tok_rows, tok_rows)
+        before, after = lax.broadcasted_iota(jnp.int32, shape, 0), lax.broadcasted_iota(jnp.int32, shape, 1)
+        earlier = ((before < after) & (quarter_of(before) == quarter_of(after))).astype(bf16)
+        experts = lax.broadcasted_iota(jnp.int32, (n_ep, tok_rows), 0)
+        ones = [(routes_ref[k : k + 1, :] == experts).astype(f32) for k in range(2)]
+        rank = jnp.dot((ones[0] + ones[1]).astype(bf16), earlier, preferred_element_type=f32)
+        return [jnp.sum(rank * one, axis=0, keepdims=True) for one in ones]
+
+    def norm_tokens():
+        step = 64
+        for i in range(tok_rows // step):
+            rows = tok_ref[i * step : (i + 1) * step, :].astype(f32)
+            normed[i * step : (i + 1) * step, :] = rms_norm(rows, mg_ref[...]).astype(bf16)
+
+    def dispatch(rank):
+        mine = quarter_of(token) == quarter
+        places = [
+            jnp.where(mine, routes_ref[k : k + 1, :].astype(f32) * cap + rank[k], -1.0) for k in range(2)
+        ]
+
+        def into(cols, rows, wide):
+            rows_out[:, :, cols] = rows.reshape(n_ep, cap, wide)
+
+        gather_rows(hit_matrix(n_ep * cap, places), into)
+
+    def own_dispatch(rank):
+        number = quarter_of(token)
+        position = lax.rem(number, 2) * 2 + number // 2
+        places = [
+            jnp.where(routes_ref[k : k + 1, :] == me, position.astype(f32) * cap + rank[k], -1.0)
+            for k in range(2)
+        ]
+
+        def into(cols, rows, wide):
+            arrived[me, :, :, :, cols] = rows.reshape(2, 2, cap, wide)
+
+        gather_rows(hit_matrix(4 * cap, places), into)
+
+    def combine_matrices(rank):
+        slot = lax.broadcasted_iota(jnp.int32, (n_ep * cap, part_rows), 0).astype(f32)
+        weighted = jnp.zeros((n_ep * cap, part_rows), f32)
+        for k in range(2):
+            place = own_part(routes_ref[k : k + 1, :].astype(f32) * cap + rank[k])
+            weighted += jnp.where(slot == place, own_part(rw_ref[k : k + 1, :]), 0.0)
+        upper = weighted.astype(bf16)
+        hits[0] = upper
+        hits[1] = (weighted - upper.astype(f32)).astype(bf16)
+
+    for copy in loads[:4]:
+        copy.wait()
+    rank = ranks()
+    norm_tokens()
+    dispatch(rank)
     pl.semaphore_wait(barrier, n_ep + 1)
 
     def ep_copy(s, t):
@@ -525,9 +574,17 @@
         block = lat_all.at[k, y if hop == 0 else 1 - y, core]
         return remote(block, block, ll_send.at[hop, k], ll_recv.at[hop, k], partner)
 
+    def tables():
+        half_dim = rope_dim // 2
+        places = lax.broadcasted_iota(jnp.int32, (tok_rows, half_dim), 0) + me * tok_rows
+        angles = places.astype(f32) * freq_ref[...]
+        cos_ref[...] = jnp.cos(angles)
+        sin_ref[...] = jnp.sin(angles)
+
     def lat_own():
         latent = rms_norm(kv_ref[...].astype(f32), lg_ref[...]).astype(bf16)
-        rot = rotate(rms_norm(rk_ref[...].astype(f32), rg_ref[...]), cos_ref[...], sin_ref[...]).astype(bf16)
+        raw = jnp.transpose(rk_ref[...].astype(f32))
+        rot = rotate(rms_norm(raw, rg_ref[...]), cos_ref[...], sin_ref[...]).astype(bf16)
         half = tok_rows // 2
         width = latent.shape[1]
         for core in range(2):
@@ -679,17 +736,38 @@
                 final_buf[j] = value
                 rep_copy(s, 1).start()
 
-    lax.fori_loop(0, 4, own_dispatch, 0)
+    def order(i):
+        if n_z % 2:
+            return i
+        return jnp.where(i < n_z - 1, lax.rem(2 * i, n_z - 1), n_z - 1)
+
+    def lat_hop(k):
+        if k < n_z:
+            lat_step(k, 0)
+
+    def attend_step(k):
+        if k < n_z:
+            if k > 0:
+                attend_line(k)
+            attend_side(k)
+
+    own_dispatch(rank)
+    combine_matrices(rank)
+    each(0, forward)
+    for copy in loads[4:]:
+        copy.wait()
+    tables()
     lat_own()
+    forward(order(1), 0)
     queries()
     attend_block(z, y, True)
 
-    def stage(s, carry):
-        each(s, forward)
+    def stage(i, carry):
+        s = order(i)
         each(s, forward_low)
         each(s, arrive)
 
-        @pl.when(s == 0)
+        @pl.when(i == 0)
         def _():
             for copy in weight_copies():
                 copy.wait()
@@ -697,23 +775,42 @@
         expert(s)
         for t in range(2):
             rlow_copy(s, t).start()
-        pl.when(s > 0)(lambda: reduce_low(s - 1))
-        pl.when(s > 1)(lambda: reduce_high(s - 2))
+
+        @pl.when(i == 0)
+        def _():
+            forward(order(1), 1)
+            each(order(2), forward)
+
+        @pl.when((i > 0) & (i < n_z - 2))
+        def _():
+            reduce_low(s)
+            each(order(i + 2), forward)
+
+        @pl.when(i == n_z - 2)
+        def _():
+            lat_hop(1)
+            reduce_low(s)
+
+        @pl.when((i > 1) & (i < n_z - 1))
+        def _():
+            reduce_high(order(i - 1))
+
         return carry
 
     lax.fori_loop(0, n_z, stage, 0)
-    lax.fori_loop(1, n_z, lat_step, 0)
-    reduce_low(n_z - 1)
-    reduce_high(n_z - 2)
-    lax.fori_loop(0, n_z, lat_side, 0)
-    reduce_high(n_z - 1)
-
-    def attend_step(k, carry):
-        pl.when(k > 0)(lambda: attend_line(k))
-        attend_side(k)
-        return carry
-
-    lax.fori_loop(0, n_z, attend_step, 0)
+    lat_hop(2)
+    last = order(n_z - 1)
+    reduce_low(last)
+    reduce_low(0)
+    tail = [order(n_z - 2), last, 0]
+    for k in range(n_z):
+        lat_side(k, 0)
+        if k == 1:
+            for far in range(3, n_z):
+                lat_hop(far)
+        if 0 < k and tail:
+            reduce_high(tail.pop(0))
+        attend_step(k)
     for head in range(heads):
         mixed = rms_norm(acc[head] / den[head], og_ref[...])
         att_ref[:, head * value_dim : (head + 1) * value_dim] = mixed.astype(bf16)
@@ -723,12 +820,12 @@
         return carry
 
     lax.fori_loop(0, n_z, returned, 0)
-    weights = rw_ref[pl.ds(pl.multiple_of(quarter * part_rows, part_rows), part_rows), :]
     wide = 512
+    lined = (((0,), (0,)), ((), ()))
     for n in range(model_dim // wide):
         values = ret[:, :, n * wide : (n + 1) * wide].reshape(n_ep * cap, wide)
-        mixed = jnp.dot(hits[0], values, preferred_element_type=f32) * weights[:, 0:1]
-        mixed += jnp.dot(hits[1], values, preferred_element_type=f32) * weights[:, 1:2]
+        mixed = lax.dot_general(hits[0], values, lined, preferred_element_type=f32)
+        mixed += lax.dot_general(hits[1], values, lined, preferred_element_type=f32)
         moe_ref[:, n * wide : (n + 1) * wide] = mixed.astype(bf16)
 
     def sent(s, carry):
@@ -759,7 +856,7 @@
 
 
 def layer(
-    queries, kv_latent, rope_key, rot_cos, rot_sin, latent_gain, w_key_up, w_value_up, query_gain, key_gain,
+    queries, kv_latent, rope_key, latent_gain, w_key_up, w_value_up, query_gain, key_gain,
     rope_gain, out_gain, moe_tokens, moe_gain, routes, route_weights, w_gate, w_up, w_down, n_ep, cap,
 ):
     tok_rows = queries.shape[0]
@@ -771,21 +868,27 @@
     n_z = n_ep // 2
     width = kv_latent.shape[1] + rope_dim
     dma = pltpu.SemaphoreType.DMA
-    kind = jnp.bfloat16
+    kind, f32 = jnp.bfloat16, jnp.float32
     pairs = (n_z, 2)
     block = (cap, model_dim)
-    vmem, anywhere = pl.BlockSpec(memory_space=VMEM), pl.BlockSpec(memory_space=pl.ANY)
+    freqs = 1.0 / THETA ** (jnp.arange(0, rope_dim, 2, dtype=f32) / rope_dim)
+    small = (
+        moe_tokens, moe_gain.reshape(1, -1), routes.T, route_weights.T, kv_latent, rope_key.T,
+        freqs.reshape(1, -1), latent_gain.reshape(1, -1), rope_gain.reshape(1, -1), queries,
+        query_gain.reshape(1, -1), w_key_up, w_value_up, key_gain.reshape(1, -1), out_gain.reshape(1, -1),
+    )
     return pl.pallas_call(
         functools.partial(layer_kernel, n_ep, heads, nope_dim, rope_dim, value_dim),
         out_shape=(
             jax.ShapeDtypeStruct((tok_rows, heads * value_dim), kind),
             jax.ShapeDtypeStruct((part_rows, model_dim), kind),
         ),
-        in_specs=[vmem] * 16 + [anywhere] * 3,
-        out_specs=(vmem, vmem),
-        scratch_shapes=[
+        in_specs=[pl.BlockSpec(memory_space=pltpu.HBM)] * (len(small) + 3),
+        out_specs=(pl.BlockSpec(memory_space=VMEM),) * 2,
+        scratch_shapes=[VMEM(array.shape, array.dtype) for array in small] + [
             VMEM((model_dim, 2 * ff), kind),
             VMEM((ff, model_dim), kind),
+            VMEM((tok_rows, model_dim), kind),
             VMEM((n_ep,) + block, kind),
             VMEM((n_ep, 2, 2) + block, kind),
             VMEM((8 * cap, ff), kind),
@@ -795,12 +898,15 @@
             VMEM((n_ep,) + block, kind),
             VMEM((n_ep,) + block, kind),
             VMEM((n_ep,) + block, kind),
-            VMEM((2, part_rows, n_ep * cap), kind),
+            VMEM((2, n_ep * cap, part_rows), kind),
             VMEM((n_z, 2, 2, tok_rows // 2, width), kind),
+            VMEM((tok_rows, rope_dim // 2), f32),
+            VMEM((tok_rows, rope_dim // 2), f32),
             VMEM((heads, tok_rows, nope_dim), kind),
             VMEM((heads, tok_rows, rope_dim), kind),
-            VMEM((heads, tok_rows, value_dim), jnp.float32),
-            VMEM((heads, tok_rows, 1), jnp.float32),
+            VMEM((heads, tok_rows, value_dim), f32),
+            VMEM((heads, tok_rows, 1), f32),
+            dma((len(small),)),
             dma((2 * (ff // LANES) + 1,)),
             dma(pairs), dma(pairs), dma(pairs), dma(pairs), dma((2,) + pairs), dma((2,) + pairs),
             dma(pairs), dma(pairs), dma(pairs), dma(pairs), dma(pairs), dma(pairs),
@@ -810,11 +916,7 @@
             collective_id=2, has_side_effects=True, vmem_limit_bytes=62 << 20
         ),
         name="layer",
-    )(
-        queries, kv_latent, rope_key, rot_cos, rot_sin, latent_gain.reshape(1, -1), w_key_up, w_value_up,
-        query_gain.reshape(1, -1), key_gain.reshape(1, -1), rope_gain.reshape(1, -1), out_gain.reshape(1, -1),
-        moe_tokens, moe_gain.reshape(1, -1), routes, route_weights, w_gate, w_up, w_down,
-    )
+    )(*small, w_gate, w_up, w_down)
 
 
 def on_device(
@@ -852,11 +954,11 @@
     experts = n_ep * w_gate.shape[0]
     capacity = (3 * top_count * part_rows + 2 * experts - 1) // (2 * experts)
     one_kernel = quarters == 4 and n_ep % 2 == 0 and w_gate.shape[0] == 1 and top_count == 2
+    one_kernel = one_kernel and n_ep >= 8
     if one_kernel and capacity % 8 == 0 and w_down.shape[1] % LANES == 0 and model_dim % 512 == 0:
         return layer(
-            queries, kv_latent, rope_key, rot_cos, rot_sin, latent_gain, w_key_up, w_value_up, query_gain,
-            key_gain, rope_gain, out_gain, moe_tokens, moe_gain, routes, route_weights, w_gate, w_up, w_down,
-            n_ep, capacity,
+            queries, kv_latent, rope_key, latent_gain, w_key_up, w_value_up, query_gain, key_gain, rope_gain,
+            out_gain, moe_tokens, moe_gain, routes, route_weights, w_gate, w_up, w_down, n_ep, capacity,
         )
     lat_part = tok_rows // quarters
 

time: 105 us -> 75.6 us (0.72)
  Pallas kernels: 94.8 us -> 71 us
  local copies, waits for them, and re-layouts: 7.66 us -> 3.24 us
    pallas_call x1, Pallas kernels: 94.8 us -> 71 us  [layer(): pl.pallas_call(functools.partial(layer_kernel, n_ep, heads, nope_dim, rop...]
    unnamed x5 -> x2, local copies, waits for them, and re-layouts: 7.66 us -> 3.24 us
    sin x1 -> x0, other arithmetic: 1.23 us -> none  [rope_tables(): return (jnp.cos(angles), jnp.sin(angles))]
where the time goes in v2:
time: 75.6 us; the launch traced here: 75.4 us
  Pallas kernels  71 us (94%)
  local copies, waits for them, and re-layouts  3.24 us (4%)
    pallas_call x1, Pallas kernels, layer(): pl.pallas_call(functools.partial(layer_kernel, n_ep, heads, nope_dim, rop...  71 us
    unnamed x2, local copies, waits for them, and re-layouts  3.24 us

profile of v2, /device:TPU:0, one launch (start us, length us, event | category | flops | bytes accessed | tf_op | source)
XLA Modules:
  0.0 75.4 jit_solution(14463687120604153512)
XLA Ops:
  0.6 0.5 negate_power_fusion.freq_hbm
  1.2 71.0 %layer.1 = (bf16[256,256]{1,0:T(8,128)(2,1)}, bf16[64,2048]{1,0:T(8,128)(2,1)}) custom-call(bf16[256,2048]{1,0:T(8,128)(2,1)} %tok_hbm.1, f32[1,2048]{1,0:T(1,128)} %bitcast.10, s32[2,256]{1,0:T(2,128)} %bitcast.11, f32[2,256]{1,0:T(2,128)} %bitcast.12, bf16[256,512]{1,0:T(8,128)(2,1)} %kv_hbm.1, bf16[64,256]{1,0:T(8,128)(2,1)} %bitcast.9, ...), custom_call_target="tpu_custom_call" | custom-call | tf_op jit(solution)/shard_map/layer/pallas_call | solution.py:880
  72.1 1.6 %copy.21 = bf16[256,256]{1,0:T(8,128)(2,1)} copy(bf16[256,256]{1,0:T(8,128)(2,1)} %get-tuple-element.4) | data formatting | bytes 262144
  73.7 1.7 %copy.22 = bf16[64,2048]{1,0:T(8,128)(2,1)} copy(bf16[64,2048]{1,0:T(8,128)(2,1)} %get-tuple-element.5) | data formatting | bytes 524288

commit v3 on v2

--- a/solution.py
+++ b/solution.py
@@ -3,6 +3,7 @@
 
 import jax
 import jax.numpy as jnp
+import numpy as np
 from jax import lax
 from jax.experimental import pallas as pl
 from jax.experimental.pallas import tpu as pltpu
@@ -401,6 +402,7 @@
     tok_rows = tok_ref.shape[0]
     part_rows = tok_rows // 4
     ff = wd.shape[0]
+    half = tok_rows // 2
     barrier = pltpu.get_barrier_semaphore()
 
     def hello(device):
@@ -556,8 +558,17 @@
         each(s, lambda s, t: ep_copy(s, t).start())
         return carry
 
-    lax.fori_loop(1, n_z, start_ep, 0)
+    def order(i):
+        if n_z % 2:
+            return i
+        return jnp.where(i < n_z - 1, lax.rem(2 * i, n_z - 1), n_z - 1)
+
+    def send_rows(i):
+        if i < n_z:
+            start_ep(order(i), 0)
+
     start_ep(0, 0)
+    send_rows(1)
 
 
     def lat_copy_z(k):
@@ -585,11 +596,15 @@
         latent = rms_norm(kv_ref[...].astype(f32), lg_ref[...]).astype(bf16)
         raw = jnp.transpose(rk_ref[...].astype(f32))
         rot = rotate(rms_norm(raw, rg_ref[...]), cos_ref[...], sin_ref[...]).astype(bf16)
-        half = tok_rows // 2
-        width = latent.shape[1]
+        step = lat_all.shape[3] - half
         for core in range(2):
-            lat_all[z, y, core, :, :width] = latent[core * half : (core + 1) * half]
-            lat_all[z, y, core, :, width:] = rot[core * half : (core + 1) * half]
+            lat_all[z, y, core, :half] = latent[core * half : (core + 1) * half]
+            first = core * half
+            lat_all[z, y, core, half:] = jnp.concatenate(
+                [rot[first + i : first + i + step] for i in range(0, half, step)], axis=1
+            )
+
+    def lat_send():
         pl.when(z < n_z - 1)(lambda: lat_copy_z(z).start())
         pl.when(y == 0)(lambda: lat_copy_y(z, y).start())
 
@@ -627,9 +642,15 @@
     scale = (nope_dim + rope_dim) ** (-0.5)
 
     def attend_block(zj, yj, own):
-        block = lat_all[zj, yj].reshape(tok_rows, lat_all.shape[-1])
-        width = block.shape[1] - rope_dim
-        latent, rot_key = block[:, :width], block[:, width:]
+        latent = lat_all[zj, yj, :, :half].reshape(tok_rows, lat_all.shape[-1])
+        rot_key = jnp.concatenate(
+            [
+                lat_all[zj, yj, core, half:, i : i + rope_dim]
+                for core in range(2)
+                for i in range(0, lat_all.shape[-1], rope_dim)
+            ],
+            axis=0,
+        )
         keys = jnp.dot(latent, wk_ref[...], preferred_element_type=f32)
         values = jnp.dot(latent, wv_ref[...], preferred_element_type=f32).astype(bf16)
         lined = (((1,), (1,)), ((), ()))
@@ -680,13 +701,16 @@
         low_copy(s, t, 0, high, 1 - low).wait_recv()
         low_copy(s, t, 1, 1 - high, 1 - low).wait_recv()
 
-    def expert(s):
+    def expert_up(s):
         first = lax.rem(z + n_z - s, n_z) * 2
         rows = arrived[pl.ds(first, 2)].reshape(8 * cap, model_dim)
         for i in range(ff // LANES):
             both = jnp.dot(rows, wgu[:, TILE * i : TILE * (i + 1)], preferred_element_type=f32)
             gate, upward = both[:, :LANES], both[:, LANES:]
             hid[:, LANES * i : LANES * (i + 1)] = (jax.nn.silu(gate) * upward).astype(bf16)
+
+    def expert_down(s):
+        first = lax.rem(z + n_z - s, n_z) * 2
         for n in range(model_dim // TILE):
             down = jnp.dot(hid[...], wd[:, TILE * n : TILE * (n + 1)], preferred_element_type=f32)
             part[pl.ds(first, 2), :, :, :, TILE * n : TILE * (n + 1)] = down.astype(bf16).reshape(
@@ -709,37 +733,25 @@
         j = ep_to(s, t)
         return remote(final_buf.at[j], ret.at[j], rep_send.at[s, t], rep_recv.at[s, t], (j, quarter))
 
-    def reduce_low(s):
-        for t in range(2):
-            j = ep_from(s, t)
-            rlow_copy(s, t).wait_recv()
-            sum_buf[j] = (part[j, low, 1 - high].astype(f32) + low_buf[j, 1 - high].astype(f32)).astype(bf16)
-            rhigh_copy(s, t).start()
-
-    def reduce_high(s):
-        for t in range(2):
-            j = ep_from(s, t)
-            rhigh_copy(s, t).wait_recv()
-            value = part[j, low, high].astype(f32) + low_buf[j, high].astype(f32) + high_buf[j].astype(f32)
-            value = value.astype(bf16)
-            if t == 0:
-
-                @pl.when(s == 0)
-                def _():
-                    ret[me] = value
-
-                @pl.when(s > 0)
-                def _():
-                    final_buf[j] = value
-                    rep_copy(s, 0).start()
-            else:
-                final_buf[j] = value
-                rep_copy(s, 1).start()
-
-    def order(i):
-        if n_z % 2:
-            return i
-        return jnp.where(i < n_z - 1, lax.rem(2 * i, n_z - 1), n_z - 1)
+    def reduce_low(s, t):
+        j = ep_from(s, t)
+        rlow_copy(s, t).wait_recv()
+        sum_buf[j] = (part[j, low, 1 - high].astype(f32) + low_buf[j, 1 - high].astype(f32)).astype(bf16)
+        rhigh_copy(s, t).start()
+
+    def reduce_high(s, t):
+        j = ep_from(s, t)
+        rhigh_copy(s, t).wait_recv()
+        value = part[j, low, high].astype(f32) + low_buf[j, high].astype(f32) + high_buf[j].astype(f32)
+        if isinstance(s, int) and s + t == 0:
+            ret[me] = value.astype(bf16)
+        else:
+            final_buf[j] = value.astype(bf16)
+            rep_copy(s, t).start()
+
+    def both(body, s):
+        body(s, 0)
+        body(s, 1)
 
     def lat_hop(k):
         if k < n_z:
@@ -753,63 +765,79 @@
 
     own_dispatch(rank)
     combine_matrices(rank)
-    each(0, forward)
     for copy in loads[4:]:
         copy.wait()
     tables()
+    forward(0, 1)
     lat_own()
-    forward(order(1), 0)
     queries()
     attend_block(z, y, True)
+
+    before, between, after = {}, {}, {}
+
+    def at(table, i, body, *args):
+        table.setdefault(i, []).append(functools.partial(body, *args))
+
+    def weights_here():
+        for copy in weight_copies():
+            copy.wait()
+
+    last = n_z - 1
+    at(before, 0, weights_here)
+    at(before, 0, send_rows, 2)
+    at(between, 0, lambda: both(forward, order(1)))
+    for i in range(3, n_z):
+        at(after, 0, send_rows, i)
+    at(after, 0, lambda: both(forward, order(2)))
+    at(before, 1, lat_send)
+    for i in range(1, last):
+        if i + 2 <= last:
+            at(between, i, lambda i=i: both(forward, order(i + 2)))
+        if i == last - 1:
+            at(after, i, lat_hop, 1)
+        at(after, i, lambda i=i: both(reduce_low, order(i)))
+
+    def run(table, i):
+        for place, bodies in table.items():
+
+            @pl.when(i == place)
+            def _():
+                for body in bodies:
+                    body()
 
     def stage(i, carry):
         s = order(i)
         each(s, forward_low)
         each(s, arrive)
-
-        @pl.when(i == 0)
-        def _():
-            for copy in weight_copies():
-                copy.wait()
-
-        expert(s)
+        run(before, i)
+        expert_up(s)
+        run(between, i)
+        expert_down(s)
         for t in range(2):
             rlow_copy(s, t).start()
-
-        @pl.when(i == 0)
-        def _():
-            forward(order(1), 1)
-            each(order(2), forward)
-
-        @pl.when((i > 0) & (i < n_z - 2))
-        def _():
-            reduce_low(s)
-            each(order(i + 2), forward)
-
-        @pl.when(i == n_z - 2)
-        def _():
-            lat_hop(1)
-            reduce_low(s)
-
-        @pl.when((i > 1) & (i < n_z - 1))
-        def _():
-            reduce_high(order(i - 1))
-
+        run(after, i)
         return carry
 
     lax.fori_loop(0, n_z, stage, 0)
+    for i in range(1, last - 1):
+        both(reduce_high, order(i))
+    both(reduce_low, order(last))
+    both(reduce_low, 0)
     lat_hop(2)
-    last = order(n_z - 1)
-    reduce_low(last)
-    reduce_low(0)
-    tail = [order(n_z - 2), last, 0]
-    for k in range(n_z):
+    lat_side(0, 0)
+    attend_step(0)
+    both(reduce_high, order(last - 1))
+    lat_side(1, 0)
+    attend_step(1)
+    for far in range(3, n_z):
+        lat_hop(far)
+    both(reduce_high, order(last))
+    lat_side(2, 0)
+    attend_step(2)
+    reduce_high(0, 1)
+    reduce_high(0, 0)
+    for k in range(3, n_z):
         lat_side(k, 0)
-        if k == 1:
-            for far in range(3, n_z):
-                lat_hop(far)
-        if 0 < k and tail:
-            reduce_high(tail.pop(0))
         attend_step(k)
     for head in range(heads):
         mixed = rms_norm(acc[head] / den[head], og_ref[...])
@@ -866,12 +894,12 @@
     part_rows = tok_rows // 4
     ff = w_down.shape[1]
     n_z = n_ep // 2
-    width = kv_latent.shape[1] + rope_dim
+    packed = tok_rows // 2 * rope_dim // kv_latent.shape[1]
     dma = pltpu.SemaphoreType.DMA
     kind, f32 = jnp.bfloat16, jnp.float32
     pairs = (n_z, 2)
     block = (cap, model_dim)
-    freqs = 1.0 / THETA ** (jnp.arange(0, rope_dim, 2, dtype=f32) / rope_dim)
+    freqs = (1.0 / THETA ** (np.arange(0, rope_dim, 2) / rope_dim)).astype(np.float32)
     small = (
         moe_tokens, moe_gain.reshape(1, -1), routes.T, route_weights.T, kv_latent, rope_key.T,
         freqs.reshape(1, -1), latent_gain.reshape(1, -1), rope_gain.reshape(1, -1), queries,
@@ -880,8 +908,8 @@
     return pl.pallas_call(
         functools.partial(layer_kernel, n_ep, heads, nope_dim, rope_dim, value_dim),
         out_shape=(
-            jax.ShapeDtypeStruct((tok_rows, heads * value_dim), kind),
-            jax.ShapeDtypeStruct((part_rows, model_dim), kind),
+            VMEM((tok_rows, heads * value_dim), kind),
+            VMEM((part_rows, model_dim), kind),
         ),
         in_specs=[pl.BlockSpec(memory_space=pltpu.HBM)] * (len(small) + 3),
         out_specs=(pl.BlockSpec(memory_space=VMEM),) * 2,
@@ -899,7 +927,7 @@
             VMEM((n_ep,) + block, kind),
             VMEM((n_ep,) + block, kind),
             VMEM((2, n_ep * cap, part_rows), kind),
-            VMEM((n_z, 2, 2, tok_rows // 2, width), kind),
+            VMEM((n_z, 2, 2, tok_rows // 2 + packed, kv_latent.shape[1]), kind),
             VMEM((tok_rows, rope_dim // 2), f32),
             VMEM((tok_rows, rope_dim // 2), f32),
             VMEM((heads, tok_rows, nope_dim), kind),
@@ -954,7 +982,9 @@
     experts = n_ep * w_gate.shape[0]
     capacity = (3 * top_count * part_rows + 2 * experts - 1) // (2 * experts)
     one_kernel = quarters == 4 and n_ep % 2 == 0 and w_gate.shape[0] == 1 and top_count == 2
-    one_kernel = one_kernel and n_ep >= 8
+    lat_parts = kv_latent.shape[1] // rope_dim
+    one_kernel = one_kernel and n_ep >= 8 and kv_latent.shape[1] % LANES == 0
+    one_kernel = one_kernel and kv_latent.shape[1] % rope_dim == 0 and n_rows % (32 * lat_parts) == 0
     if one_kernel and capacity % 8 == 0 and w_down.shape[1] % LANES == 0 and model_dim % 512 == 0:
         return layer(
             queries, kv_latent, rope_key, latent_gain, w_key_up, w_value_up, query_gain, key_gain, rope_gain,

time: 75.6 us -> 61.9 us (0.82)
  Pallas kernels: 71 us -> 59.7 us
  local copies, waits for them, and re-layouts: 3.24 us -> 1.36 us
    pallas_call x1, Pallas kernels: 71 us -> 59.7 us  [layer(): pl.pallas_call(functools.partial(layer_kernel, n_ep, heads, nope_dim, rop...]
    unnamed x2, local copies, waits for them, and re-layouts: 3.24 us -> 1.36 us
where the time goes in v3:
time: 61.9 us; the launch traced here: 61.7 us
  Pallas kernels  59.7 us (96%)
  local copies, waits for them, and re-layouts  1.36 us (2%)
  between operations  0.65 us (1%)
    pallas_call x1, Pallas kernels, layer(): pl.pallas_call(functools.partial(layer_kernel, n_ep, heads, nope_dim, rop...  59.7 us
    unnamed x2, local copies, waits for them, and re-layouts  1.36 us

profile of v3, /device:TPU:0, one launch (start us, length us, event | category | flops | bytes accessed | tf_op | source)
XLA Modules:
  0.0 61.7 jit_solution(11466268836468108922)
XLA Ops:
  0.6 59.7 %layer.1 = (bf16[256,256]{1,0:T(8,128)(2,1)S(1)}, bf16[64,2048]{1,0:T(8,128)(2,1)S(1)}) custom-call(bf16[256,2048]{1,0:T(8,128)(2,1)} %tok_hbm.1, f32[1,2048]{1,0:T(1,128)} %bitcast.10, s32[2,256]{1,0:T(2,128)} %bitcast.11, f32[2,256]{1,0:T(2,128)} %bitcast.12, bf16[256,512]{1,0:T(8,128)(2,1)} %kv_hbm.1, bf16[64,256]{1,0:T(8,128)(2,1)} %bitcast.9, ...), custom_call_target="tpu_custom_call" | custom-call | tf_op jit(solution)/shard_map/layer/pallas_call | solution.py:908
  60.4 0.7 %copy.22 = bf16[256,256]{1,0:T(8,128)(2,1)} copy(bf16[256,256]{1,0:T(8,128)(2,1)S(1)} %get-tuple-element.2) | data formatting | bytes 262144
  61.0 0.7 %copy.23 = bf16[64,2048]{1,0:T(8,128)(2,1)} copy(bf16[64,2048]{1,0:T(8,128)(2,1)S(1)} %get-tuple-element.3) | data formatting | bytes 524288

commit v4 on v3

--- a/solution.py
+++ b/solution.py
@@ -438,9 +438,6 @@
     ]
     for copy in loads:
         copy.start()
-    for copy in weight_copies():
-        copy.start()
-
     def ep_to(s, t):
         return lax.rem(z + s, n_z) * 2 + lax.rem(y + t, 2)
 
@@ -522,6 +519,8 @@
 
     for copy in loads[:4]:
         copy.wait()
+    for copy in weight_copies():
+        copy.start()
     rank = ranks()
     norm_tokens()
     dispatch(rank)
@@ -773,7 +772,7 @@
     queries()
     attend_block(z, y, True)
 
-    before, between, after = {}, {}, {}
+    first, before, between, after = {}, {}, {}, {}
 
     def at(table, i, body, *args):
         table.setdefault(i, []).append(functools.partial(body, *args))
@@ -788,14 +787,20 @@
     at(between, 0, lambda: both(forward, order(1)))
     for i in range(3, n_z):
         at(after, 0, send_rows, i)
-    at(after, 0, lambda: both(forward, order(2)))
-    at(before, 1, lat_send)
+    at(first, 1, lambda: both(forward, order(2)))
+    at(after, 0, lat_send)
     for i in range(1, last):
         if i + 2 <= last:
-            at(between, i, lambda i=i: both(forward, order(i + 2)))
-        if i == last - 1:
-            at(after, i, lat_hop, 1)
+            at(between, i, lambda i=i: forward(order(i + 2), 0))
+            at(between, i + 1, lambda i=i: forward(order(i + 2), 1))
         at(after, i, lambda i=i: both(reduce_low, order(i)))
+        if i > 1:
+            at(after, i, lambda i=i: both(reduce_high, order(i - 1)))
+    at(after, 1, lat_hop, 1)
+    at(after, 2, lat_hop, 2)
+    at(between, last, reduce_low, 0, 1)
+    at(between, last, lat_side, 0, 0)
+    at(between, last, lat_side, 1, 0)
 
     def run(table, i):
         for place, bodies in table.items():
@@ -808,6 +813,7 @@
     def stage(i, carry):
         s = order(i)
         each(s, forward_low)
+        run(first, i)
         each(s, arrive)
         run(before, i)
         expert_up(s)
@@ -819,26 +825,21 @@
         return carry
 
     lax.fori_loop(0, n_z, stage, 0)
-    for i in range(1, last - 1):
-        both(reduce_high, order(i))
     both(reduce_low, order(last))
-    both(reduce_low, 0)
-    lat_hop(2)
-    lat_side(0, 0)
+    reduce_low(0, 0)
+    both(reduce_high, order(last - 1))
     attend_step(0)
-    both(reduce_high, order(last - 1))
-    lat_side(1, 0)
     attend_step(1)
+    lat_side(2, 0)
     for far in range(3, n_z):
         lat_hop(far)
     both(reduce_high, order(last))
-    lat_side(2, 0)
-    attend_step(2)
     reduce_high(0, 1)
     reduce_high(0, 0)
-    for k in range(3, n_z):
-        lat_side(k, 0)
-        attend_step(k)
+    for far in range(3, n_z):
+        lat_side(far, 0)
+    for far in range(2, n_z):
+        attend_step(far)
     for head in range(heads):
         mixed = rms_norm(acc[head] / den[head], og_ref[...])
         att_ref[:, head * value_dim : (head + 1) * value_dim] = mixed.astype(bf16)

time: 61.9 us -> 60.2 us (0.973)
  the two profiles are of different devices: /device:TPU:0 before, /device:TPU:24 now
where the time goes in v4:
time: 60.2 us; the launch traced here: 60.1 us
  Pallas kernels  58.1 us (97%)
  local copies, waits for them, and re-layouts  1.36 us (2%)
  between operations  0.65 us (1%)
    pallas_call x1, Pallas kernels, layer(): pl.pallas_call(functools.partial(layer_kernel, n_ep, heads, nope_dim, rop...  58.1 us
    unnamed x2, local copies, waits for them, and re-layouts  1.36 us

profile of v4, /device:TPU:24, one launch (start us, length us, event | category | flops | bytes accessed | tf_op | source)
XLA Modules:
  0.0 60.1 jit_solution(2304602560233622662)
XLA Ops:
  0.6 58.1 %layer.1 = (bf16[256,256]{1,0:T(8,128)(2,1)S(1)}, bf16[64,2048]{1,0:T(8,128)(2,1)S(1)}) custom-call(bf16[256,2048]{1,0:T(8,128)(2,1)} %tok_hbm.1, f32[1,2048]{1,0:T(1,128)} %bitcast.10, s32[2,256]{1,0:T(2,128)} %bitcast.11, f32[2,256]{1,0:T(2,128)} %bitcast.12, bf16[256,512]{1,0:T(8,128)(2,1)} %kv_hbm.1, bf16[64,256]{1,0:T(8,128)(2,1)} %bitcast.9, ...), custom_call_target="tpu_custom_call" | custom-call | tf_op jit(solution)/shard_map/layer/pallas_call | solution.py:909
  58.7 0.7 %copy.22 = bf16[256,256]{1,0:T(8,128)(2,1)} copy(bf16[256,256]{1,0:T(8,128)(2,1)S(1)} %get-tuple-element.2) | data formatting | bytes 262144
  59.4 0.7 %copy.23 = bf16[64,2048]{1,0:T(8,128)(2,1)} copy(bf16[64,2048]{1,0:T(8,128)(2,1)S(1)} %get-tuple-element.3) | data formatting | bytes 524288
